TPU v7x, 32 devices: a whole 2x2x4 slice. The times are simulated.
32 devices in a mesh: ep: 32 (over z, y, x, core).
Axes of the slice: x: 2, y: 2, z: 4, core: 2. Of those that a mesh axis runs over, the one named last changes fastest.
Arguments:
- tokens: bfloat16 [512, 1024], P('ep'), may hold values from -6 to 6
- lengths: int32 [512], P('ep'), may hold values from 1 to 8191
- cache_keys: bfloat16 [512, 128, 512], P('ep'), may hold values from -6 to 6
- cache_values: bfloat16 [512, 128, 1024], P('ep'), may hold values from -6 to 6
- retention_state: float32 [512, 4, 128, 256], P('ep'), may hold values from -24 to 24
- mix_gain: float32 [1024], replicated, may hold values from 0.1 to 1.9
- query_weight: bfloat16 [1024, 512], replicated, may hold values from -0.1875 to 0.1875
- key_weight: bfloat16 [1024, 512], replicated, may hold values from -0.1875 to 0.1875
- value_weight: bfloat16 [1024, 1024], replicated, may hold values from -0.1875 to 0.1875
- out_weight: bfloat16 [1024, 1024], replicated, may hold values from -0.1875 to 0.1875
- ffn_gain: float32 [1024], replicated, may hold values from 0.1 to 1.9
- routes: int32 [512, 6], P('ep'), may hold values from 0 to 31, all different within a row; in each aligned block of 16 rows (0 to 15, 16 to 31, ...) at most 8 rows name the same one
- route_scores: float32 [512, 6], P('ep'), may hold values from 0.05 to 1
- expert_gate: bfloat16 [32, 1024, 256], P('ep'), may hold values from -0.1875 to 0.1875
- expert_up: bfloat16 [32, 1024, 256], P('ep'), may hold values from -0.1875 to 0.1875
- expert_down: bfloat16 [32, 256, 1024], P('ep'), may hold values from -0.375 to 0.375
- shared_gate: bfloat16 [1024, 256], replicated, may hold values from -0.1875 to 0.1875
- shared_up: bfloat16 [1024, 256], replicated, may hold values from -0.1875 to 0.1875
- shared_down: bfloat16 [256, 1024], replicated, may hold values from -0.375 to 0.375
- dense_gate: bfloat16 [4096, 1024], P('ep'), may hold values from -0.1875 to 0.1875
- dense_up: bfloat16 [4096, 1024], P('ep'), may hold values from -0.1875 to 0.1875
- dense_down: bfloat16 [4096, 1024], P('ep'), may hold values from -0.09375 to 0.09375
- dense_mix: float32 [1024], replicated, may hold values from -3 to 3
Outputs:
- layer_out: bfloat16 [512, 1024], P('ep')
- new_keys: bfloat16 [512, 512], P('ep')
- new_values: bfloat16 [512, 1024], P('ep')
Inputs may be any that keep to these rules, and one draw needn't show every extreme that they name: `routes`: each row names 6 different experts; among the rows of one device no expert is named more than 8 times.
All inputs are finite; a program needn't handle non-finite values.
Results may differ from a plain program's by a relative error of at most 0.012.
Values may be sent and summed in bfloat16 or wider, within the bound.
A program may use at most 128 MiB of HBM per device.

v0:
```python
import functools
import math

import jax
import jax.numpy as jnp
from jax import lax
from jax.experimental import pallas as pl
from jax.experimental.pallas import tpu as pltpu
from jax.sharding import PartitionSpec as P

eps = 1e-06
route_scale = 2.5
rope_base = 10000.0


def normed(values):
    return values * lax.rsqrt(jnp.mean(values * values, axis=-1, keepdims=True) + eps)


def log_decay(head_count):
    return jnp.log1p(-jnp.exp2(-5.0 - jnp.arange(head_count, dtype=jnp.float32)))


def rotate(values, positions):
    half_size = values.shape[-1] // 2
    inverse = rope_base ** (-jnp.arange(half_size, dtype=jnp.float32) / half_size)
    angles = positions.astype(jnp.float32)[:, None, None] * inverse[None, None, :]
    cosine = jnp.cos(angles)
    sine_part = jnp.sin(angles)
    first_half = values[..., :half_size]
    second = values[..., half_size:]
    return jnp.concatenate(
        [first_half * cosine - second * sine_part, first_half * sine_part + second * cosine],
        axis=-1,
    )


def retain(
    tokens, lengths, mix_gain, w_query, w_key, w_value, w_out, cache_keys, cache_values, carry_state
):
    seq_count, head_count, key_size, value_size = carry_state.shape
    block_size = cache_keys.shape[1]
    widened = tokens.astype(jnp.float32)
    normal_in = (normed(widened) * mix_gain).astype(jnp.bfloat16)
    raw_query = jnp.dot(normal_in, w_query, preferred_element_type=jnp.float32).reshape(
        seq_count, head_count, key_size
    )
    raw_key = jnp.dot(normal_in, w_key, preferred_element_type=jnp.float32).reshape(
        seq_count, head_count, key_size
    )
    raw_value = jnp.dot(normal_in, w_value, preferred_element_type=jnp.float32).reshape(
        seq_count, head_count, value_size
    )
    queries = (rotate(raw_query, lengths) * key_size ** (-0.5)).astype(jnp.bfloat16)
    new_keys = rotate(raw_key, lengths).astype(jnp.bfloat16)
    new_values = raw_value.astype(jnp.bfloat16)
    filled = lengths % block_size
    decay_rate = log_decay(head_count)
    places = jnp.arange(block_size, dtype=jnp.int32)
    stored_keys = cache_keys.reshape(seq_count, block_size, head_count, key_size)
    stored_values = cache_values.reshape(seq_count, block_size, head_count, value_size)
    scores = jnp.einsum("shd,sjhd->shj", queries, stored_keys, preferred_element_type=jnp.float32)
    distance = jnp.maximum(filled[:, None] - places[None, :], 0).astype(jnp.float32)
    live_mask = places[None, :] < filled[:, None]
    weighted = jnp.where(
        live_mask[:, None, :],
        scores * jnp.exp(distance[:, None, :] * decay_rate[None, :, None]),
        0.0,
    ).astype(jnp.bfloat16)
    own_weight = jnp.sum(
        queries.astype(jnp.float32) * new_keys.astype(jnp.float32), axis=-1
    ).astype(jnp.bfloat16)
    inside = jnp.einsum(
        "shj,sjhe->she", weighted, stored_values, preferred_element_type=jnp.float32
    )
    inside = inside + own_weight.astype(jnp.float32)[:, :, None] * new_values.astype(jnp.float32)
    carried = jnp.einsum(
        "shd,shde->she", queries.astype(jnp.float32), carry_state, precision=lax.Precision.HIGHEST
    )
    carried = (
        carried
        * jnp.exp((filled.astype(jnp.float32)[:, None] + 1.0) * decay_rate[None, :])[:, :, None]
    )
    headed = (
        normed(inside + carried).astype(jnp.bfloat16).reshape(seq_count, head_count * value_size)
    )
    mixer_out = jnp.dot(headed, w_out, preferred_element_type=jnp.float32)
    residual = widened + normed(mixer_out)
    return (
        residual,
        new_keys.reshape(seq_count, head_count * key_size),
        new_values.reshape(seq_count, head_count * value_size),
    )


f32 = jnp.float32
bf16 = jnp.bfloat16


def slice_dims(device_count):
    side = max(1, math.isqrt(device_count // 8))
    return device_count // (2 * side * side), side, side


def mm(a, b):
    return lax.dot_general(a, b, (((1,), (0,)), ((), ())), preferred_element_type=f32)


def mm_t(a, b):
    return lax.dot_general(a, b, (((1,), (1,)), ((), ())), preferred_element_type=f32)


def silu(v):
    return v / (1.0 + jnp.exp(-v))


def channel_mixer(
    dims,
    width,
    expert_count,
    block_ref,
    residual_ref,
    mix_ref,
    eg_hbm,
    eu_hbm,
    ed_hbm,
    dg_hbm,
    du_hbm,
    dd_hbm,
    sg_hbm,
    su_hbm,
    sd_hbm,
    out_ref,
    eg,
    eu,
    ed,
    dg,
    du,
    dd,
    sg,
    su,
    sd,
    gathered,
    partial,
    in_core,
    sum_core,
    in2a,
    in2b,
    sum2a,
    sum2b,
    in3a,
    in3b,
    sum3,
    in4,
    total,
    w_sem,
    own_sem,
    gz_s,
    gz_r,
    g2a_s,
    g2a_r,
    g2b_s,
    g2b_r,
    g3a_s,
    g3a_r,
    g3b_s,
    g3b_r,
    g4_s,
    g4_r,
    r1_s,
    r1_r,
    r2a_s,
    r2a_r,
    r2b_s,
    r2b_r,
    r3a_s,
    r3a_r,
    r3b_s,
    r3b_r,
    r4_s,
    r4_r,
):
    zs, ys, xs = dims
    half = width // 2
    me = lax.axis_index("ep")
    core = lax.rem(me, 2)
    x = lax.rem(me // 2, xs)
    y = lax.rem(me // (2 * xs), ys)
    z = me // (2 * xs * ys)
    other = 1 - core

    def turn(at, by, size):
        return lax.rem(at + by + size, size)

    def device(zz, yy, xx, cc):
        return ((zz * ys + yy) * xs + xx) * 2 + cc

    def z_peer(by):
        return device(turn(z, by, zs), y, x, core)

    def y_peer(by):
        return device(z, turn(y, by, ys), x, core)

    def x_peer(by):
        return device(z, y, turn(x, by, xs), core)

    mate = device(z, y, x, other)
    peers = (
        [z_peer(p) for p in range(1, zs)]
        + [y_peer(p) for p in range(1, ys)]
        + [x_peer(p) for p in range(1, xs)]
        + [mate]
    )

    loads = []
    for at, (a, b) in enumerate(
        [
            (sg_hbm, sg),
            (su_hbm, su),
            (sd_hbm, sd),
            (eg_hbm.at[0], eg),
            (eu_hbm.at[0], eu),
            (ed_hbm.at[0], ed),
            (dg_hbm, dg),
            (du_hbm, du),
            (dd_hbm, dd),
        ]
    ):
        load = pltpu.make_async_copy(a, b, w_sem.at[at])
        load.start()
        loads.append(load)
    own = pltpu.make_async_copy(block_ref, gathered.at[z, y, x, core], own_sem)
    own.start()

    barrier = pltpu.get_barrier_semaphore()
    for peer in peers:
        pl.semaphore_signal(
            barrier, inc=1, device_id=(peer,), device_id_type=pl.DeviceIdType.MESH
        )
    pl.semaphore_wait(barrier, len(peers))

    started = []

    def send(source, target, send_sem, recv_sem, peer):
        copy = pltpu.make_async_remote_copy(
            src_ref=source,
            dst_ref=target,
            send_sem=send_sem,
            recv_sem=recv_sem,
            device_id=(peer,),
            device_id_type=pl.DeviceIdType.MESH,
        )
        copy.start()
        started.append(copy)
        return copy

    own.wait()
    for_z, for2, for3, for4 = {}, {}, {}, {}
    for o in range(1, zs):
        mine = gathered.at[z, y, x, core]
        for_z[o] = send(mine, mine, gz_s.at[o - 1], gz_r.at[o - 1], z_peer(o))

    def spread2(o):
        at = turn(z, -o, zs)
        if o:
            for_z[o].wait_recv()
        a = gathered.at[at, y, x, core, :, pl.ds(0, half)]
        b = gathered.at[at, y, x, core, :, pl.ds(half, gathered.shape[-1] - half)]
        for2[o] = [
            send(a, a, g2a_s.at[o, p - 1], g2a_r.at[o, p - 1], y_peer(p)) for p in range(1, ys)
        ] + [send(b, b, g2b_s.at[o, p - 1], g2b_r.at[o, p - 1], x_peer(p)) for p in range(1, xs)]

    def spread3(o):
        at = turn(z, -o, zs)
        for copy in for2[o]:
            copy.wait_recv()
        a = gathered.at[at, :, x, core, :, pl.ds(0, half)]
        b = gathered.at[at, y, :, core, :, pl.ds(half, gathered.shape[-1] - half)]
        for3[o] = [
            send(a, a, g3a_s.at[o, p - 1], g3a_r.at[o, p - 1], x_peer(p)) for p in range(1, xs)
        ] + [send(b, b, g3b_s.at[o, p - 1], g3b_r.at[o, p - 1], y_peer(p)) for p in range(1, ys)]

    def spread4(o):
        at = turn(z, -o, zs)
        for copy in for3[o]:
            copy.wait_recv()
        a = gathered.at[at, :, :, core]
        for4[o] = send(a, a, g4_s.at[o], g4_r.at[o], mate)

    to1, to2, to3, to4 = {}, {}, {}, {}
    gate = 1.0 / (1.0 + jnp.exp(-mix_ref[...]))

    def branches(o):
        at = turn(z, -o, zs)
        if o == 0:
            for load in loads[3:]:
                load.wait()
        for4[o].wait_recv()
        rows = ys * xs * 2 * gathered.shape[4]
        block = gathered[at].reshape(rows, gathered.shape[-1])
        inputs = block[:, :width]
        extra = block[:, width:].astype(f32)
        lane = lax.broadcasted_iota(jnp.int32, extra.shape, 1)
        chosen = (lane == me) | (lane == me + expert_count)
        weight = jnp.sum(jnp.where(chosen, extra, 0.0), axis=1, keepdims=True)
        hidden = (silu(mm(inputs, eg[...])) * mm(inputs, eu[...])).astype(bf16)
        dense = (silu(mm_t(inputs, dg[...])) * mm_t(inputs, du[...])).astype(bf16)
        terms = weight * mm(hidden, ed[...]) + gate * mm(dense, dd[...])
        partial[at] = terms.astype(bf16).reshape(partial.shape[1:])
        to1[o] = send(
            partial.at[at, :, :, other], in_core.at[o], r1_s.at[o], r1_r.at[o], mate
        )

    def reduce2(o):
        at = turn(z, -o, zs)
        to1[o].wait_recv()
        sum_core[o] = (partial[at, :, :, core].astype(f32) + in_core[o].astype(f32)).astype(bf16)
        to2[o] = [
            send(
                sum_core.at[o, :, turn(x, p, xs), :, pl.ds(0, half)],
                in2a.at[o, p - 1],
                r2a_s.at[o, p - 1],
                r2a_r.at[o, p - 1],
                x_peer(p),
            )
            for p in range(1, xs)
        ] + [
            send(
                sum_core.at[o, turn(y, p, ys), :, :, pl.ds(half, width - half)],
                in2b.at[o, p - 1],
                r2b_s.at[o, p - 1],
                r2b_r.at[o, p - 1],
                y_peer(p),
            )
            for p in range(1, ys)
        ]

    def reduce3(o):
        for copy in to2[o]:
            copy.wait_recv()
        a = sum_core[o, :, x, :, 0:half].astype(f32)
        for p in range(1, xs):
            a = a + in2a[o, p - 1].astype(f32)
        sum2a[o] = a.astype(bf16)
        b = sum_core[o, y, :, :, half:width].astype(f32)
        for p in range(1, ys):
            b = b + in2b[o, p - 1].astype(f32)
        sum2b[o] = b.astype(bf16)
        to3[o] = [
            send(
                sum2a.at[o, turn(y, p, ys)],
                in3a.at[o, p - 1],
                r3a_s.at[o, p - 1],
                r3a_r.at[o, p - 1],
                y_peer(p),
            )
            for p in range(1, ys)
        ] + [
            send(
                sum2b.at[o, turn(x, p, xs)],
                in3b.at[o, p - 1],
                r3b_s.at[o, p - 1],
                r3b_r.at[o, p - 1],
                x_peer(p),
            )
            for p in range(1, xs)
        ]

    def reduce4(o):
        for copy in to3[o]:
            copy.wait_recv()
        a = sum2a[o, y].astype(f32)
        for p in range(1, ys):
            a = a + in3a[o, p - 1].astype(f32)
        b = sum2b[o, x].astype(f32)
        for p in range(1, xs):
            b = b + in3b[o, p - 1].astype(f32)
        if o == 0:
            total[:, 0:half] = total[:, 0:half] + a
            total[:, half:width] = total[:, half:width] + b
        else:
            sum3[o - 1, :, 0:half] = a.astype(bf16)
            sum3[o - 1, :, half:width] = b.astype(bf16)
            to4[o] = send(
                sum3.at[o - 1], in4.at[o - 1], r4_s.at[o - 1], r4_r.at[o - 1], z_peer(-o)
            )

    def shared():
        for load in loads[:3]:
            load.wait()
        inputs = block_ref[:, :width]
        hidden = (silu(mm(inputs, sg[...])) * mm(inputs, su[...])).astype(bf16)
        total[...] = mm(hidden, sd[...])

    stages = [spread2, spread3, spread4, branches, reduce2, reduce3, reduce4]
    for step in range(zs + len(stages) - 1):
        for at, stage in enumerate(stages):
            if 0 <= step - at < zs:
                stage(step - at)
        if step == 0:
            shared()

    combined = total[...]
    for o in range(1, zs):
        to4[o].wait_recv()
        combined = combined + in4[o - 1].astype(f32)
    scale = lax.rsqrt(jnp.mean(combined * combined, axis=-1, keepdims=True) + eps)
    out_ref[...] = (residual_ref[...] + combined * scale).astype(bf16)
    for copy in started:
        copy.wait_send()


def mixed_channels(block, residual, dense_mix, weights, expert_count, device_count):
    seq_count, width = residual.shape
    wide = block.shape[1]
    zs, ys, xs = slice_dims(device_count)
    half = width // 2
    rest = width - half
    y1, x1, z1 = max(ys - 1, 1), max(xs - 1, 1), max(zs - 1, 1)
    held = [pltpu.VMEM(w.shape[-2:], bf16) for w in weights]
    dma = pltpu.SemaphoreType.DMA
    buffers = [
        pltpu.VMEM((zs, ys, xs, 2, seq_count, wide), bf16),
        pltpu.VMEM((zs, ys, xs, 2, seq_count, width), bf16),
        pltpu.VMEM((zs, ys, xs, seq_count, width), bf16),
        pltpu.VMEM((zs, ys, xs, seq_count, width), bf16),
        pltpu.VMEM((zs, x1, ys, seq_count, half), bf16),
        pltpu.VMEM((zs, y1, xs, seq_count, rest), bf16),
        pltpu.VMEM((zs, ys, seq_count, half), bf16),
        pltpu.VMEM((zs, xs, seq_count, rest), bf16),
        pltpu.VMEM((zs, y1, seq_count, half), bf16),
        pltpu.VMEM((zs, x1, seq_count, rest), bf16),
        pltpu.VMEM((z1, seq_count, width), bf16),
        pltpu.VMEM((z1, seq_count, width), bf16),
        pltpu.VMEM((seq_count, width), f32),
    ]
    sems = [dma((len(weights),)), dma]
    for shape in [
        (z1,),
        (zs, y1),
        (zs, x1),
        (zs, x1),
        (zs, y1),
        (zs,),
        (zs,),
        (zs, x1),
        (zs, y1),
        (zs, y1),
        (zs, x1),
        (z1,),
    ]:
        sems += [dma(shape), dma(shape)]
    vmem = pl.BlockSpec(memory_space=pltpu.VMEM)
    return pl.pallas_call(
        functools.partial(channel_mixer, (zs, ys, xs), width, expert_count),
        out_shape=jax.ShapeDtypeStruct((seq_count, width), bf16),
        in_specs=[vmem] * 3 + [pl.BlockSpec(memory_space=pl.ANY)] * len(weights),
        out_specs=vmem,
        scratch_shapes=held + buffers + sems,
        compiler_params=pltpu.CompilerParams(
            collective_id=0, has_side_effects=True, vmem_limit_bytes=56 * 1024 * 1024
        ),
    )(block, residual, dense_mix.reshape(1, width), *weights)


def per_device(
    tokens,
    lengths,
    cache_keys,
    cache_values,
    retention_state,
    mix_gain,
    query_weight,
    key_weight,
    value_weight,
    out_weight,
    ffn_gain,
    routes,
    route_scores,
    expert_gate,
    expert_up,
    expert_down,
    shared_gate,
    shared_up,
    shared_down,
    dense_gate,
    dense_up,
    dense_down,
    dense_mix,
):
    residual, new_keys, new_values = retain(
        tokens,
        lengths,
        mix_gain,
        query_weight,
        key_weight,
        value_weight,
        out_weight,
        cache_keys,
        cache_values,
        retention_state,
    )
    normal_ffn = (normed(residual) * ffn_gain).astype(jnp.bfloat16)
    device_count = lax.axis_size("ep")
    expert_count = device_count * expert_gate.shape[0]
    route_weight = route_scores / jnp.sum(route_scores, axis=-1, keepdims=True) * route_scale
    named = routes[:, :, None] == jnp.arange(expert_count, dtype=jnp.int32)[None, None, :]
    by_expert = jnp.sum(jnp.where(named, route_weight[:, :, None], 0.0), axis=1)
    upper = lax.reduce_precision(by_expert, 8, 7)
    pad = -(2 * expert_count) % 128
    block = jnp.concatenate(
        [
            normal_ffn,
            upper.astype(bf16),
            (by_expert - upper).astype(bf16),
            jnp.zeros((routes.shape[0], pad), bf16),
        ],
        axis=1,
    )
    weights = (
        expert_gate,
        expert_up,
        expert_down,
        dense_gate,
        dense_up,
        dense_down,
        shared_gate,
        shared_up,
        shared_down,
    )
    layer_out = mixed_channels(block, residual, dense_mix, weights, expert_count, device_count)
    return (layer_out, new_keys, new_values)


def solution(mesh):
    in_specs = (
        P("ep", None),
        P("ep"),
        P("ep", None, None),
        P("ep", None, None),
        P("ep", None, None, None),
        P(),
        P(),
        P(),
        P(),
        P(),
        P(),
        P("ep", None),
        P("ep", None),
        P("ep", None, None),
        P("ep", None, None),
        P("ep", None, None),
        P(),
        P(),
        P(),
        P("ep", None),
        P("ep", None),
        P("ep", None),
        P(),
    )
    out_specs = (P("ep", None), P("ep", None), P("ep", None))
    return jax.shard_map(
        per_device, mesh=mesh, in_specs=in_specs, out_specs=out_specs, check_vma=False
    )
```

profile of v0, /device:TPU:0, one launch (start us, length us, event | category | flops | bytes accessed | tf_op | source)
XLA Modules:
  0.0 61.4 jit_solution(16598637189115214346)
XLA Ops:
  0.6 0.0 copy-start
  0.6 1.0 %fusion.3 = f32[16]{0:T(128)S(1)} fusion(bf16[16,1024]{1,0:T(8,128)(2,1)} %param.23), kind=kLoop, calls=%fused_computation.7 | loop fusion | flops 49136 | bytes 32832 | tf_op jit(solution)/shard_map/reduce_sum | solution.py:17
  1.7 1.6 %fusion.19 = f32[16,512]{1,0:T(8,128)S(1)} fusion(bf16[1024,512]{1,0:T(8,128)(2,1)} %param.29, bf16[16,1024]{1,0:T(8,128)(2,1)} %param.23, f32[1024]{0:T(1024)} %param.28, f32[16]{0:T(128)S(1)} %add_rsqrt_fusion.3), kind=kOutput, calls=%fused_computation.58 | convolution fusion | flops 16842752 | bytes 1118272 | tf_op jit(solution)/shard_map/dot_general | solution.py:45
  3.3 0.7 %convert_element_type.79 = f32[16]{0:T(128)S(1)} convert(s32[16]{0:T(128)} %param.24) | non-fusion elementwise | flops 16 | bytes 128 | tf_op jit(solution)/shard_map/convert_element_type | solution.py:27
  3.9 0.1 multiply_cosine_fusion
  4.1 0.1 multiply_subtract_fusion.1
  4.1 1.5 %fusion.17 = f32[16,512]{1,0:T(8,128)S(1)} fusion(bf16[1024,512]{1,0:T(8,128)(2,1)} %param.30, bf16[16,1024]{1,0:T(8,128)(2,1)} %param.23, f32[1024]{0:T(1024)} %param.28, f32[16]{0:T(128)S(1)} %add_rsqrt_fusion.3), kind=kOutput, calls=%fused_computation.57 | convolution fusion | flops 16842752 | bytes 1118272 | tf_op jit(solution)/shard_map/dot_general | solution.py:48
  5.7 0.1 multiply_subtract_fusion
  5.8 0.2 multiply_reduce_fusion.3
  6.0 3.9 %copy.35 = bf16[16,128,512]{1,2,0:T(8,128)(2,1)} copy(bf16[16,128,512]{2,1,0:T(8,128)(2,1)} %param.25) | data formatting | bytes 4194304 | tf_op jit(solution)/shard_map/reshape | solution.py:60
  9.9 0.0 copy-start.9
  9.9 2.2 %fusion.11 = f32[16,4,1,128]{3,2,1,0:T(1,128)S(1)} fusion(bf16[16,128,4,128]{1,3,2,0:T(8,128)(2,1)} %bitcast.34, bf16[16,4,128,1]{2,1,0,3:T(4,128)(2,1)S(1)} %bitcast.36), kind=kOutput, calls=%fused_computation.32 | convolution fusion | flops 2097152 | bytes 2146304 | tf_op jit(solution)/shard_map/shd,sjhd->shj/dot_general | solution.py:62
  12.2 0.0 copy-done.9
  12.2 0.1 maximum_convert_fusion.1
  12.3 0.1 iota_compare_fusion.1
  12.4 0.1 fusion.13
  12.5 2.8 %fusion = f32[16,4,1,256]{3,2,1,0:T(1,128)S(1)} fusion(bf16[16,16,4,8,256]{4,3,2,1,0:T(8,128)(2,1)} %bitcast.35, bf16[16,4,128,1]{2,1,0,3:T(4,128)(2,1)S(1)} %fusion.13), kind=kOutput, calls=%fused_computation | convolution fusion | flops 4194304 | bytes 4276224 | tf_op jit(solution)/shard_map/shj,sjhe->she/dot_general | solution.py:73
  15.3 0.0 copy-start.1
  15.3 0.0 copy-start.2
  15.3 0.0 copy-start.5
  15.3 6.3 %fusion.9 = f32[16,4,1,256]{3,2,1,0:T(1,128)S(1)} fusion(f32[16,4,128,256]{3,2,1,0:T(8,128)} %param.27, bf16[16,4,128,1]{2,1,0,3:T(4,128)(2,1)S(1)} %bitcast.37), kind=kOutput, calls=%fused_computation.30 | convolution fusion | flops 25165824 | bytes 8470528 | tf_op jit(solution)/shard_map/shd,shde->she/dot_general | solution.py:77
  21.6 0.0 copy-done.1
  21.6 0.0 copy-done.2
  21.6 0.0 copy-done.5
  21.6 0.0 copy-start.7
  21.6 0.0 copy-start.6
  21.6 0.0 copy-start.8
  21.7 0.4 convolution_convert_fusion
  22.1 0.0 copy-start.4
  22.1 0.1 multiply_exponential_fusion
  22.2 0.2 multiply_reduce_fusion.2
  22.4 0.1 multiply_convert_fusion.1
  22.5 0.0 copy-done
  22.5 0.5 multiply_reduce_fusion.1
  23.0 0.2 multiply_reduce_fusion
  23.2 0.0 copy-start.3
  23.3 0.0 copy-done.7
  23.3 0.1 multiply_convert_fusion
  23.3 0.0 copy-done.6
  23.4 0.0 copy-done.8
  23.4 0.1 select_reduce_fusion
  23.5 0.7 %concatenate.11.block_ref = bf16[16,1152]{1,0:T(8,128)(2,1)} concatenate(bf16[16,1024]{1,0:T(8,128)(2,1)S(1)} %multiply_convert_fusion, bf16[16,32]{1,0:T(8,128)(2,1)S(1)} %get-tuple-element.17, bf16[16,32]{1,0:T(8,128)(2,1)S(1)} %get-tuple-element.16, bf16[16,64]{1,0:T(8,128)(2,1)S(1)} %broadcast_in_dim.26), dimensions={1} | concatenate | bytes 73728 | tf_op jit(solution)/shard_map/concatenate | solution.py:511
  24.2 0.0 copy-done.3
  24.2 35.2 %shard_map.238 = bf16[16,1024]{1,0:T(8,128)(2,1)} custom-call(bf16[16,1152]{1,0:T(8,128)(2,1)} %concatenate.11.block_ref, f32[16,1024]{1,0:T(8,128)} %copy-done.3, f32[1,1024]{1,0:T(1,128)} %bitcast.43, bf16[1,1024,256]{2,1,0:T(8,128)(2,1)} %eg_hbm.1, bf16[1,1024,256]{2,1,0:T(8,128)(2,1)} %eu_hbm.1, bf16[1,256,1024]{2,1,0:T(8,128)(2,1)} %ed_hbm.1, ...), custom_call_target="tpu_custom_call" | custom-call | tf_op jit(solution)/shard_map/pallas_call | solution.py:454
  59.4 0.0 copy-done.4
  59.4 0.6 copy.54
  60.1 1.4 %copy.56 = bf16[16,1024]{1,0:T(8,128)(2,1)} copy(bf16[16,1024]{1,0:T(8,128)(2,1)} %shard_map.238) | data formatting | bytes 65536
  (16 shorter events, 0.2 us)
Async XLA Ops:
  0.6 21.9 %copy-start = (bf16[1024,1024]{1,0:T(8,128)(2,1)S(1)}, bf16[1024,1024]{1,0:T(8,128)(2,1)}, u32[]{:S(2)}) copy-start(bf16[1024,1024]{1,0:T(8,128)(2,1)} %param.32) | copy-start | bytes 6291460
  9.9 2.2 %copy-start.9 = (s32[16]{0:T(128)S(1)}, s32[16]{0:T(128)}, u32[]{:S(2)}) copy-start(s32[16]{0:T(128)} %param.24) | copy-start | bytes 196
  15.3 6.3 %copy-start.1 = (bf16[1024,1024]{1,0:T(8,128)(2,1)S(1)}, bf16[1024,1024]{1,0:T(8,128)(2,1)}, u32[]{:S(2)}) copy-start(bf16[1024,1024]{1,0:T(8,128)(2,1)} %param.31) | copy-start | bytes 6291460
  15.3 6.3 %copy-start.2 = (bf16[16,1024]{1,0:T(8,128)(2,1)S(1)}, bf16[16,1024]{1,0:T(8,128)(2,1)}, u32[]{:S(2)}) copy-start(bf16[16,1024]{1,0:T(8,128)(2,1)} %param.23) | copy-start | bytes 98308
  15.3 6.3 %copy-start.5 = (f32[1024]{0:T(1024)S(1)}, f32[1024]{0:T(1024)}, u32[]{:S(2)}) copy-start(f32[1024]{0:T(1024)} %param.28) | copy-start | bytes 12292
  21.6 1.6 %copy-start.7 = (f32[1024]{0:T(1024)S(1)}, f32[1024]{0:T(1024)}, u32[]{:S(2)}) copy-start(f32[1024]{0:T(1024)} %param.33) | copy-start | bytes 12292
  21.6 1.7 %copy-start.6 = (f32[16,6]{0,1:T(8,128)S(1)}, f32[16,6]{0,1:T(8,128)}, u32[]{:S(2)}) copy-start(f32[16,6]{0,1:T(8,128)} %param.35) | copy-start | bytes 1156
  21.6 1.7 %copy-start.8 = (s32[16,6]{0,1:T(8,128)S(1)}, s32[16,6]{0,1:T(8,128)}, u32[]{:S(2)}) copy-start(s32[16,6]{0,1:T(8,128)} %param.34) | copy-start | bytes 1156
  22.1 37.4 %copy-start.4 = (bf16[16,1024]{1,0:T(8,128)(2,1)}, bf16[16,1024]{1,0:T(8,128)(2,1)S(1)}, u32[]{:S(2)}) copy-start(bf16[16,1024]{1,0:T(8,128)(2,1)S(1)} %convolution_convert_fusion) | copy-start | bytes 98308
  23.2 1.0 %copy-start.3 = (f32[16,1024]{1,0:T(8,128)}, f32[16,1024]{1,0:T(8,128)S(1)}, u32[]{:S(2)}) copy-start(f32[16,1024]{1,0:T(8,128)S(1)} %get-tuple-element.4.residual_ref) | copy-start | bytes 196612
where the time goes:
time: 61.9 us; the launch traced here: 61.4 us
  Pallas kernels  35.2 us (57%)
  matrix products  15.4 us (25%)
  local copies, waits for them, and re-layouts  6.74 us (11%)
  other arithmetic  3.24 us (5%)
  between operations  0.87 us (1%)
    pallas_call x1, Pallas kernels, mixed_channels(): pl.pallas_call(functools.partial(channel_mixer, (zs, ys, xs), width, expe...  35.2 us
    dot_general x1, matrix products, retain(): jnp.einsum('shd,shde->she', queries.astype(jnp.float32), carry_state, pre...  6.26 us
    reshape x1, local copies, waits for them, and re-layouts, retain(): cache_keys.reshape(seq_count, block_size, head_count, key_size)  3.93 us
    dot_general x1, matrix products, retain(): jnp.einsum('shj,sjhe->she', weighted, stored_values, preferred_element_ty...  2.84 us
    dot_general x1, matrix products, retain(): jnp.einsum('shd,sjhd->shj', queries, stored_keys, preferred_element_type=...  2.24 us
    unnamed x23, local copies, waits for them, and re-layouts  2.04 us
    dot_general x1, matrix products, retain(): jnp.dot(normal_in, w_query, preferred_element_type=jnp.float32)  1.55 us
    dot_general x1, matrix products, retain(): jnp.dot(normal_in, w_key, preferred_element_type=jnp.float32)  1.55 us

commit v1 on v0

--- a/solution.py
+++ b/solution.py
@@ -12,102 +12,283 @@
 route_scale = 2.5
 rope_base = 10000.0
 
-
-def normed(values):
-    return values * lax.rsqrt(jnp.mean(values * values, axis=-1, keepdims=True) + eps)
-
-
-def log_decay(head_count):
-    return jnp.log1p(-jnp.exp2(-5.0 - jnp.arange(head_count, dtype=jnp.float32)))
-
-
-def rotate(values, positions):
-    half_size = values.shape[-1] // 2
-    inverse = rope_base ** (-jnp.arange(half_size, dtype=jnp.float32) / half_size)
-    angles = positions.astype(jnp.float32)[:, None, None] * inverse[None, None, :]
-    cosine = jnp.cos(angles)
-    sine_part = jnp.sin(angles)
-    first_half = values[..., :half_size]
-    second = values[..., half_size:]
-    return jnp.concatenate(
-        [first_half * cosine - second * sine_part, first_half * sine_part + second * cosine],
-        axis=-1,
-    )
-
-
-def retain(
-    tokens, lengths, mix_gain, w_query, w_key, w_value, w_out, cache_keys, cache_values, carry_state
-):
-    seq_count, head_count, key_size, value_size = carry_state.shape
-    block_size = cache_keys.shape[1]
-    widened = tokens.astype(jnp.float32)
-    normal_in = (normed(widened) * mix_gain).astype(jnp.bfloat16)
-    raw_query = jnp.dot(normal_in, w_query, preferred_element_type=jnp.float32).reshape(
-        seq_count, head_count, key_size
-    )
-    raw_key = jnp.dot(normal_in, w_key, preferred_element_type=jnp.float32).reshape(
-        seq_count, head_count, key_size
-    )
-    raw_value = jnp.dot(normal_in, w_value, preferred_element_type=jnp.float32).reshape(
-        seq_count, head_count, value_size
-    )
-    queries = (rotate(raw_query, lengths) * key_size ** (-0.5)).astype(jnp.bfloat16)
-    new_keys = rotate(raw_key, lengths).astype(jnp.bfloat16)
-    new_values = raw_value.astype(jnp.bfloat16)
-    filled = lengths % block_size
-    decay_rate = log_decay(head_count)
-    places = jnp.arange(block_size, dtype=jnp.int32)
-    stored_keys = cache_keys.reshape(seq_count, block_size, head_count, key_size)
-    stored_values = cache_values.reshape(seq_count, block_size, head_count, value_size)
-    scores = jnp.einsum("shd,sjhd->shj", queries, stored_keys, preferred_element_type=jnp.float32)
-    distance = jnp.maximum(filled[:, None] - places[None, :], 0).astype(jnp.float32)
-    live_mask = places[None, :] < filled[:, None]
-    weighted = jnp.where(
-        live_mask[:, None, :],
-        scores * jnp.exp(distance[:, None, :] * decay_rate[None, :, None]),
-        0.0,
-    ).astype(jnp.bfloat16)
-    own_weight = jnp.sum(
-        queries.astype(jnp.float32) * new_keys.astype(jnp.float32), axis=-1
-    ).astype(jnp.bfloat16)
-    inside = jnp.einsum(
-        "shj,sjhe->she", weighted, stored_values, preferred_element_type=jnp.float32
-    )
-    inside = inside + own_weight.astype(jnp.float32)[:, :, None] * new_values.astype(jnp.float32)
-    carried = jnp.einsum(
-        "shd,shde->she", queries.astype(jnp.float32), carry_state, precision=lax.Precision.HIGHEST
-    )
-    carried = (
-        carried
-        * jnp.exp((filled.astype(jnp.float32)[:, None] + 1.0) * decay_rate[None, :])[:, :, None]
-    )
-    headed = (
-        normed(inside + carried).astype(jnp.bfloat16).reshape(seq_count, head_count * value_size)
-    )
-    mixer_out = jnp.dot(headed, w_out, preferred_element_type=jnp.float32)
-    residual = widened + normed(mixer_out)
-    return (
-        residual,
-        new_keys.reshape(seq_count, head_count * key_size),
-        new_values.reshape(seq_count, head_count * value_size),
-    )
-
-
 f32 = jnp.float32
 bf16 = jnp.bfloat16
+lanes = 128
+
+
+def inverse_rms(values):
+    return lax.rsqrt(jnp.mean(values * values, axis=-1, keepdims=True) + eps)
+
+
+def mm(a, b):
+    return lax.dot_general(a, b, (((1,), (0,)), ((), ())), preferred_element_type=f32)
+
+
+def mm_t(a, b):
+    return lax.dot_general(a, b, (((1,), (1,)), ((), ())), preferred_element_type=f32)
+
+
+def cos_sin(angles):
+    turn = jnp.floor(angles * (2.0 / math.pi) + 0.5)
+    r = angles - turn * 1.5703125
+    r = r - turn * 4.837512969970703125e-4
+    r = r - turn * 7.54978995489188216e-8
+    z = r * r
+    sine = ((-1.9515295891e-4 * z + 8.3321608736e-3) * z - 1.6666654611e-1) * z * r + r
+    cosine = ((2.443315711809948e-5 * z - 1.388731625493765e-3) * z + 4.166664568298827e-2) * z * z
+    cosine = cosine - 0.5 * z + 1.0
+    quarter = turn - 4.0 * jnp.floor(turn * 0.25)
+    odd = (quarter == 1.0) | (quarter == 3.0)
+    c = jnp.where(odd, sine, cosine)
+    s = jnp.where(odd, cosine, sine)
+    c = jnp.where((quarter == 1.0) | (quarter == 2.0), -c, c)
+    s = jnp.where(quarter >= 2.0, -s, s)
+    return c, s
+
+
+def to_columns(row, count):
+    return jnp.transpose(jnp.broadcast_to(row, (lanes, lanes)))[0:count]
+
+
+def route_block(routes, weight, top_k, expert_count, wide, count):
+    tiles = []
+    for at in range(0, wide, lanes):
+        place = at + lax.broadcasted_iota(jnp.int32, (lanes, lanes), 0)
+        lower = place >= expert_count
+        expert = jnp.where(lower, place - expert_count, place)
+        named = jnp.zeros((lanes, lanes), f32)
+        for k in range(top_k):
+            named = named + jnp.where(expert == routes[k : k + 1], weight[k : k + 1], 0.0)
+        upper = named.astype(bf16).astype(f32)
+        kept = jnp.where(lower, named - upper, upper)
+        tiles.append(jnp.transpose(kept)[0:count].astype(bf16))
+    return tiles
+
+
+def mixer(
+    head_count,
+    expert_count,
+    tokens_ref,
+    lengths_ref,
+    routes_ref,
+    scores_ref,
+    mix_ref,
+    ffn_ref,
+    wq_hbm,
+    wk_hbm,
+    wv_hbm,
+    wo_hbm,
+    keys_hbm,
+    values_hbm,
+    state_hbm,
+    residual_ref,
+    block_ref,
+    new_keys_ref,
+    new_values_ref,
+    wq,
+    wk,
+    wv,
+    wo,
+    keys,
+    values,
+    state,
+    weights,
+    headed,
+    small,
+    w_sem,
+    k_sem,
+    v_sem,
+    s_sem,
+):
+    seq_count, block_size, key_width = keys.shape
+    key_size = key_width // head_count
+    width = tokens_ref.shape[1]
+    value_width = values.shape[2]
+    value_size = value_width // head_count
+    pairs = seq_count // 2
+
+    def load(source, target, sem):
+        copy = pltpu.make_async_copy(source, target, sem)
+        copy.start()
+        return copy
+
+    get_q = load(wq_hbm, wq, w_sem.at[0])
+    get_k = load(wk_hbm, wk, w_sem.at[1])
+    get_keys = [
+        load(keys_hbm.at[pl.ds(2 * p, 2)], keys.at[pl.ds(2 * p, 2)], k_sem.at[p])
+        for p in range(pairs)
+    ]
+    get_v = load(wv_hbm, wv, w_sem.at[2])
+    get_values, get_state = [], []
+    for p in range(pairs):
+        part = pl.ds(2 * p, 2)
+        get_values.append(load(values_hbm.at[part], values.at[part], v_sem.at[p]))
+        get_state.append(load(state_hbm.at[part], state.at[part], s_sem.at[p]))
+    get_o = load(wo_hbm, wo, w_sem.at[3])
+
+    widened = tokens_ref[...].astype(f32)
+    normal_in = (widened * inverse_rms(widened) * mix_ref[...]).astype(bf16)
+
+    top_k = routes_ref.shape[0]
+    small[...] = jnp.zeros_like(small)
+    small[0, 0:1, 0:seq_count] = lengths_ref[...].astype(f32)
+    small[1, 0:top_k, 0:seq_count] = routes_ref[...].astype(f32)
+    scores = scores_ref[...]
+    small[2, 0:top_k, 0:seq_count] = (
+        scores / jnp.sum(scores, axis=0, keepdims=True) * route_scale
+    )
+    positions = to_columns(small[0, 0:1], seq_count)
+    lane = lax.broadcasted_iota(jnp.int32, (seq_count, lanes), 1)
+    row = lax.broadcasted_iota(jnp.int32, (seq_count, lanes), 0)
+    half = key_size // 2
+    entry = jnp.where(lane < half, lane, lane - half).astype(f32)
+    inverse = jnp.exp(entry * (-math.log(rope_base) / half))
+    cosine, sine = cos_sin(positions * inverse)
+    signed = jnp.where(lane < half, -sine, sine)
+    filled = positions - block_size * jnp.floor(positions * (1.0 / block_size))
+    distance = filled - lane.astype(f32)
+    live = distance > 0.0
+    rates = [math.log1p(-(2.0 ** (-5 - h))) for h in range(head_count)]
+    decay = [
+        jnp.where(live, jnp.exp(jnp.maximum(distance, 0.0) * rate), 0.0) for rate in rates
+    ]
+
+    def rotated(raw):
+        return raw * cosine + pltpu.roll(raw, half, 1) * signed
+
+    tiles = route_block(
+        small[1].astype(jnp.int32),
+        small[2],
+        top_k,
+        expert_count,
+        block_ref.shape[1] - width,
+        seq_count,
+    )
+    for at, tile in enumerate(tiles):
+        block_ref[:, width + at * lanes : width + (at + 1) * lanes] = tile
+
+    get_q.wait()
+    raw_query = mm(normal_in, wq[...])
+    get_k.wait()
+    raw_key = mm(normal_in, wk[...])
+    queries, own = [], []
+    for h in range(head_count):
+        part = slice(h * key_size, (h + 1) * key_size)
+        query = (rotated(raw_query[:, part]) * key_size ** (-0.5)).astype(bf16)
+        key = rotated(raw_key[:, part]).astype(bf16)
+        new_keys_ref[:, part] = key
+        queries.append(query)
+        weight = jnp.sum(query.astype(f32) * key.astype(f32), axis=1, keepdims=True)
+        own.append(weight.astype(bf16).astype(f32))
+
+    rows = 2 * block_size
+    for p in range(pairs):
+        get_keys[p].wait()
+        for h in range(head_count):
+            stored = keys[2 * p : 2 * p + 2, :, h * key_size : (h + 1) * key_size]
+            scores = mm_t(queries[h], stored.reshape(rows, key_size))
+            for i in range(2):
+                part = scores[:, i * block_size : (i + 1) * block_size] * decay[h]
+                weights[h, :, p * rows + i * block_size : p * rows + (i + 1) * block_size] = (
+                    jnp.where(row == 2 * p + i, part, 0.0).astype(bf16)
+                )
+
+    get_v.wait()
+    new_values = mm(normal_in, wv[...]).astype(bf16)
+    new_values_ref[...] = new_values
+
+    inside = [jnp.zeros((seq_count, value_size), f32) for _ in range(head_count)]
+    carried = [jnp.zeros((seq_count, value_size), f32) for _ in range(head_count)]
+    zero = jnp.zeros((seq_count, key_size), bf16)
+    for p in range(pairs):
+        get_values[p].wait()
+        for h in range(head_count):
+            stored = values[2 * p : 2 * p + 2, :, h * value_size : (h + 1) * value_size]
+            inside[h] = inside[h] + mm(
+                weights[h, :, p * rows : (p + 1) * rows], stored.reshape(rows, value_size)
+            )
+        get_state[p].wait()
+        for h in range(head_count):
+            chosen = jnp.concatenate(
+                [jnp.where(row == 2 * p + i, queries[h].astype(f32), 0.0) for i in range(2)],
+                axis=1,
+            ).astype(bf16)
+            held = state[2 * p : 2 * p + 2, h].reshape(2 * key_size, value_size)
+            carried[h] = carried[h] + mm(chosen, held.astype(bf16))
+
+    for h in range(head_count):
+        part = slice(h * value_size, (h + 1) * value_size)
+        fade = jnp.exp((filled[:, 0:1] + 1.0) * rates[h])
+        retained = inside[h] + own[h] * new_values[:, part].astype(f32) + carried[h] * fade
+        headed[:, part] = (retained * inverse_rms(retained)).astype(bf16)
+    get_o.wait()
+    mixer_out = mm(headed[...], wo[...])
+    residual = widened + mixer_out * inverse_rms(mixer_out)
+    residual_ref[...] = residual
+    block_ref[:, 0:width] = (residual * inverse_rms(residual) * ffn_ref[...]).astype(bf16)
+
+
+def mixed_sequences(
+    tokens,
+    lengths,
+    routes,
+    route_scores,
+    mix_gain,
+    ffn_gain,
+    matrices,
+    cache_keys,
+    cache_values,
+    retention_state,
+    expert_count,
+):
+    seq_count, width = tokens.shape
+    head_count = retention_state.shape[1]
+    extra = 2 * expert_count
+    extra += -extra % lanes
+    held = [pltpu.VMEM(w.shape, w.dtype) for w in matrices]
+    held += [pltpu.VMEM(w.shape, w.dtype) for w in (cache_keys, cache_values, retention_state)]
+    dma = pltpu.SemaphoreType.DMA
+    vmem = pl.BlockSpec(memory_space=pltpu.VMEM)
+    anywhere = pl.BlockSpec(memory_space=pl.ANY)
+    return pl.pallas_call(
+        functools.partial(mixer, head_count, expert_count),
+        out_shape=[
+            jax.ShapeDtypeStruct((seq_count, width), f32),
+            jax.ShapeDtypeStruct((seq_count, width + extra), bf16),
+            jax.ShapeDtypeStruct((seq_count, cache_keys.shape[2]), bf16),
+            jax.ShapeDtypeStruct((seq_count, cache_values.shape[2]), bf16),
+        ],
+        in_specs=[vmem] * 6 + [anywhere] * 7,
+        out_specs=[vmem] * 4,
+        scratch_shapes=held
+        + [
+            pltpu.VMEM((head_count, seq_count, seq_count * cache_keys.shape[1]), bf16),
+            pltpu.VMEM((seq_count, cache_values.shape[2]), bf16),
+            pltpu.VMEM((3, 8, lanes), f32),
+            dma((4,)),
+            dma((seq_count // 2,)),
+            dma((seq_count // 2,)),
+            dma((seq_count // 2,)),
+        ],
+        compiler_params=pltpu.CompilerParams(vmem_limit_bytes=56 * 1024 * 1024),
+    )(
+        tokens,
+        lengths.reshape(1, seq_count),
+        routes.T,
+        route_scores.T,
+        mix_gain.reshape(1, width),
+        ffn_gain.reshape(1, width),
+        *matrices,
+        cache_keys,
+        cache_values,
+        retention_state,
+    )
 
 
 def slice_dims(device_count):
     side = max(1, math.isqrt(device_count // 8))
     return device_count // (2 * side * side), side, side
-
-
-def mm(a, b):
-    return lax.dot_general(a, b, (((1,), (0,)), ((), ())), preferred_element_type=f32)
-
-
-def mm_t(a, b):
-    return lax.dot_general(a, b, (((1,), (1,)), ((), ())), preferred_element_type=f32)
 
 
 def silu(v):
@@ -488,34 +669,20 @@
     dense_down,
     dense_mix,
 ):
-    residual, new_keys, new_values = retain(
+    device_count = lax.axis_size("ep")
+    expert_count = device_count * expert_gate.shape[0]
+    residual, block, new_keys, new_values = mixed_sequences(
         tokens,
         lengths,
+        routes,
+        route_scores,
         mix_gain,
-        query_weight,
-        key_weight,
-        value_weight,
-        out_weight,
+        ffn_gain,
+        (query_weight, key_weight, value_weight, out_weight),
         cache_keys,
         cache_values,
         retention_state,
-    )
-    normal_ffn = (normed(residual) * ffn_gain).astype(jnp.bfloat16)
-    device_count = lax.axis_size("ep")
-    expert_count = device_count * expert_gate.shape[0]
-    route_weight = route_scores / jnp.sum(route_scores, axis=-1, keepdims=True) * route_scale
-    named = routes[:, :, None] == jnp.arange(expert_count, dtype=jnp.int32)[None, None, :]
-    by_expert = jnp.sum(jnp.where(named, route_weight[:, :, None], 0.0), axis=1)
-    upper = lax.reduce_precision(by_expert, 8, 7)
-    pad = -(2 * expert_count) % 128
-    block = jnp.concatenate(
-        [
-            normal_ffn,
-            upper.astype(bf16),
-            (by_expert - upper).astype(bf16),
-            jnp.zeros((routes.shape[0], pad), bf16),
-        ],
-        axis=1,
+        expert_count,
     )
     weights = (
         expert_gate,

time: 61.9 us -> 47.9 us (0.77)
  matrix products: 15.4 us -> 0 us
  Pallas kernels: 35.2 us -> 45.6 us
  local copies, waits for them, and re-layouts: 6.74 us -> 1.38 us
  other arithmetic: 3.24 us -> 0 us
    dot_general x7 -> x0, matrix products: 15.4 us -> none  [the longest x1 6.26 us: retain(): jnp.einsum('shd,shde->she', queries.astype(jnp.float32), carry_state, pre...]
    pallas_call x0 -> x1, Pallas kernels: none -> 10.4 us  [mixed_sequences(): pl.pallas_call(functools.partial(mixer, head_count, expert_count), out_sh...]
    reshape x3 -> x0, local copies, waits for them, and re-layouts: 3.96 us -> none  [the longest x1 3.93 us: retain(): cache_keys.reshape(seq_count, block_size, head_count, key_size)]
    reduce_sum x6 -> x0, other arithmetic: 1.71 us -> none  [the longest x3 1.41 us: normed(): jnp.mean(values * values, axis=-1, keepdims=True) + eps]
    convert_element_type x7 -> x0, other arithmetic: 1 us -> none  [the longest x1 0.66 us: rotate(): positions.astype(jnp.float32)[:, None, None] * inverse[None, None, :]]
    concatenate x1 -> x0, local copies, waits for them, and re-layouts: 0.7 us -> none  [per_device(): jnp.concatenate([normal_ffn, upper.astype(bf16), (by_expert - upper).asty...]
    unnamed x23 -> x1, local copies, waits for them, and re-layouts: 2.04 us -> 1.38 us
where the time goes in v1:
time: 47.9 us; the launch traced here: 47.6 us
  Pallas kernels  45.6 us (95%)
  local copies, waits for them, and re-layouts  1.38 us (3%)
  between operations  0.65 us (1%)
    pallas_call x1, Pallas kernels, mixed_channels(): pl.pallas_call(functools.partial(channel_mixer, (zs, ys, xs), width, expe...  35.2 us
    pallas_call x1, Pallas kernels, mixed_sequences(): pl.pallas_call(functools.partial(mixer, head_count, expert_count), out_sh...  10.4 us
    unnamed x1, local copies, waits for them, and re-layouts  1.38 us

profile of v1, /device:TPU:0, one launch (start us, length us, event | category | flops | bytes accessed | tf_op | source)
XLA Modules:
  0.0 47.6 jit_solution(14663672760894942994)
XLA Ops:
  0.6 10.4 %shard_map.238 = (f32[16,1024]{1,0:T(8,128)}, bf16[16,1152]{1,0:T(8,128)(2,1)}, bf16[16,512]{1,0:T(8,128)(2,1)}, bf16[16,1024]{1,0:T(8,128)(2,1)}) custom-call(bf16[16,1024]{1,0:T(8,128)(2,1)} %tokens_ref.1, s32[1,16]{1,0:T(1,128)} %bitcast.11, s32[6,16]{1,0:T(8,128)} %bitcast.7, f32[6,16]{1,0:T(8,128)} %bitcast.8, f32[1,1024]{1,0:T(1,128)} %bitcast.9, ...), custom_call_target="tpu_custom_call" | custom-call | tf_op jit(solution)/shard_map/pallas_call | solution.py:254
  11.0 35.2 %shard_map.239 = bf16[16,1024]{1,0:T(8,128)(2,1)} custom-call(bf16[16,1152]{1,0:T(8,128)(2,1)} %get-tuple-element.7.block_ref, f32[16,1024]{1,0:T(8,128)} %get-tuple-element.8.residual_ref, f32[1,1024]{1,0:T(1,128)} %bitcast.6, bf16[1,1024,256]{2,1,0:T(8,128)(2,1)} %eg_hbm.1, bf16[1,1024,256]{2,1,0:T(8,128)(2,1)} %eu_hbm.1, bf16[1,256,1024]{2,1,0:T(8,128)(2,1)} %ed_hbm.1, ...), custom_call_target="tpu_custom_call" | custom-call | tf_op jit(solution)/shard_map/pallas_call | solution.py:635
  46.2 1.4 %copy.27 = bf16[16,1024]{1,0:T(8,128)(2,1)} copy(bf16[16,1024]{1,0:T(8,128)(2,1)} %shard_map.239) | data formatting | bytes 65536

commit v2 on v1

v2 whole, which is shorter than its diff:
```python
import functools
import math

import jax
import jax.numpy as jnp
from jax import lax
from jax.experimental import pallas as pl
from jax.experimental.pallas import tpu as pltpu
from jax.sharding import PartitionSpec as P

eps = 1e-06
route_scale = 2.5
rope_base = 10000.0

f32 = jnp.float32
bf16 = jnp.bfloat16
lanes = 128


def inverse_rms(values):
    return lax.rsqrt(jnp.mean(values * values, axis=-1, keepdims=True) + eps)


def mm(a, b):
    return lax.dot_general(a, b, (((1,), (0,)), ((), ())), preferred_element_type=f32)


def mm_t(a, b):
    return lax.dot_general(a, b, (((1,), (1,)), ((), ())), preferred_element_type=f32)


def cos_sin(angles):
    turn = jnp.floor(angles * (2.0 / math.pi) + 0.5)
    r = angles - turn * 1.5703125
    r = r - turn * 4.837512969970703125e-4
    r = r - turn * 7.54978995489188216e-8
    z = r * r
    sine = ((-1.9515295891e-4 * z + 8.3321608736e-3) * z - 1.6666654611e-1) * z * r + r
    cosine = ((2.443315711809948e-5 * z - 1.388731625493765e-3) * z + 4.166664568298827e-2) * z * z
    cosine = cosine - 0.5 * z + 1.0
    quarter = turn - 4.0 * jnp.floor(turn * 0.25)
    odd = (quarter == 1.0) | (quarter == 3.0)
    c = jnp.where(odd, sine, cosine)
    s = jnp.where(odd, cosine, sine)
    c = jnp.where((quarter == 1.0) | (quarter == 2.0), -c, c)
    s = jnp.where(quarter >= 2.0, -s, s)
    return c, s


def to_columns(row, count):
    return jnp.transpose(jnp.broadcast_to(row, (lanes, lanes)))[0:count]


def route_block(routes, weight, top_k, expert_count, wide, count):
    tiles = []
    for at in range(0, wide, lanes):
        place = at + lax.broadcasted_iota(jnp.int32, (lanes, lanes), 0)
        lower = place >= expert_count
        expert = jnp.where(lower, place - expert_count, place)
        named = jnp.zeros((lanes, lanes), f32)
        for k in range(top_k):
            named = named + jnp.where(expert == routes[k : k + 1], weight[k : k + 1], 0.0)
        upper = named.astype(bf16).astype(f32)
        kept = jnp.where(lower, named - upper, upper)
        tiles.append(jnp.transpose(kept)[0:count].astype(bf16))
    return tiles


def silu(v):
    return v / (1.0 + jnp.exp(-v))


def slice_dims(device_count):
    side = max(1, math.isqrt(device_count // 8))
    return device_count // (2 * side * side), side, side


def crossed(at, by):
    moved, bit = at, 1
    while bit <= by:
        if by & bit:
            moved = moved + bit - 2 * bit * lax.rem(at // bit, 2)
        bit *= 2
    return moved


def layer(
    dims,
    head_count,
    expert_count,
    tokens_ref,
    lengths_ref,
    routes_ref,
    scores_ref,
    mix_ref,
    ffn_ref,
    dense_ref,
    wq_hbm,
    wk_hbm,
    wv_hbm,
    wo_hbm,
    keys_hbm,
    values_hbm,
    state_hbm,
    eg_hbm,
    eu_hbm,
    ed_hbm,
    dg_hbm,
    du_hbm,
    dd_hbm,
    sg_hbm,
    su_hbm,
    sd_hbm,
    out_ref,
    new_keys_ref,
    new_values_ref,
    wq,
    wk,
    wv,
    wo,
    keys,
    values,
    state,
    eg,
    eu,
    ed,
    dg,
    du,
    dd,
    sg,
    su,
    sd,
    weights,
    headed,
    small,
    extras,
    gathered,
    partial,
    arrived,
    summed,
    returned,
    w_sem,
    k_sem,
    v_sem,
    s_sem,
    f_sem,
    swap_s,
    swap_r,
    ez_s,
    ez_r,
    ep_s,
    ep_r,
    z_s,
    z_r,
    d_s,
    d_r,
    p_s,
    p_r,
    b_s,
    b_r,
):
    seq_count, block_size, key_width = keys.shape
    key_size = key_width // head_count
    width = tokens_ref.shape[1]
    value_width = values.shape[2]
    value_size = value_width // head_count
    pairs = seq_count // 2

    zs, ys, xs = dims
    me = lax.axis_index("ep")
    core = lax.rem(me, 2)
    x = lax.rem(me // 2, xs)
    y = lax.rem(me // (2 * xs), ys)
    z = me // (2 * xs * ys)
    paired = zs & (zs - 1) == 0

    def device(zz, yy, xx, cc):
        return ((zz * ys + yy) * xs + xx) * 2 + cc

    def source(o):
        return crossed(z, o) if paired else lax.rem(z - o + zs, zs)

    def target(o):
        return crossed(z, o) if paired else lax.rem(z + o, zs)

    around = [(dy, dx) for dy in range(ys) for dx in range(xs) if dy or dx]

    def beside(i):
        dy, dx = around[i]
        return lax.rem(y + dy, ys), lax.rem(x + dx, xs)

    mate = device(z, y, x, 1 - core)
    z_peers = [device(target(o), y, x, core) for o in range(1, zs)]
    home_peers = [device(source(o), y, x, core) for o in range(1, zs)]
    plane_peers = [device(z, *beside(i), core) for i in range(len(around))]

    def load(origin, place, sem):
        copy = pltpu.make_async_copy(origin, place, sem)
        copy.start()
        return copy

    get_q = load(wq_hbm, wq, w_sem.at[0])
    get_k = load(wk_hbm, wk, w_sem.at[1])
    get_keys = [
        load(keys_hbm.at[pl.ds(2 * p, 2)], keys.at[pl.ds(2 * p, 2)], k_sem.at[p])
        for p in range(pairs)
    ]
    get_ffn = [
        load(origin, place, f_sem.at[at])
        for at, (origin, place) in enumerate(
            [
                (eg_hbm, eg.at[pl.ds(0, 1)]),
                (eu_hbm, eu.at[pl.ds(0, 1)]),
                (ed_hbm, ed.at[pl.ds(0, 1)]),
                (dg_hbm, dg.at[0]),
                (du_hbm, du.at[0]),
                (dd_hbm, dd.at[0]),
            ]
        )
    ]
    get_v = load(wv_hbm, wv, w_sem.at[2])
    get_values, get_state = [], []
    for p in range(pairs):
        part = pl.ds(2 * p, 2)
        get_values.append(load(values_hbm.at[part], values.at[part], v_sem.at[p]))
        get_state.append(load(state_hbm.at[part], state.at[part], s_sem.at[p]))
    get_o = load(wo_hbm, wo, w_sem.at[3])
    get_shared = [
        load(origin, place, f_sem.at[6 + at])
        for at, (origin, place) in enumerate([(sg_hbm, sg), (su_hbm, su), (sd_hbm, sd)])
    ]

    barrier = pltpu.get_barrier_semaphore()
    peers = z_peers + plane_peers + [mate]
    if not paired:
        peers = peers + home_peers
    for peer in peers:
        pl.semaphore_signal(
            barrier, inc=1, device_id=(peer,), device_id_type=pl.DeviceIdType.MESH
        )

    started = []

    def send(origin, place, send_sem, recv_sem, peer):
        copy = pltpu.make_async_remote_copy(
            src_ref=origin,
            dst_ref=place,
            send_sem=send_sem,
            recv_sem=recv_sem,
            device_id=(peer,),
            device_id_type=pl.DeviceIdType.MESH,
        )
        copy.start()
        started.append(copy)
        return copy

    widened = tokens_ref[...].astype(f32)
    normal_in = (widened * inverse_rms(widened) * mix_ref[...]).astype(bf16)

    top_k = routes_ref.shape[0]
    small[...] = jnp.zeros_like(small)
    small[0, 0:1, 0:seq_count] = lengths_ref[...].astype(f32)
    small[1, 0:top_k, 0:seq_count] = routes_ref[...].astype(f32)
    scores = scores_ref[...]
    small[2, 0:top_k, 0:seq_count] = (
        scores / jnp.sum(scores, axis=0, keepdims=True) * route_scale
    )
    tiles = route_block(
        small[1].astype(jnp.int32),
        small[2],
        top_k,
        expert_count,
        extras.shape[-1],
        seq_count,
    )
    for at, tile in enumerate(tiles):
        extras[z, y, x, :, at * lanes : (at + 1) * lanes] = tile

    positions = to_columns(small[0, 0:1], seq_count)
    lane = lax.broadcasted_iota(jnp.int32, (seq_count, lanes), 1)
    row = lax.broadcasted_iota(jnp.int32, (seq_count, lanes), 0)
    half = key_size // 2
    entry = jnp.where(lane < half, lane, lane - half).astype(f32)
    inverse = jnp.exp(entry * (-math.log(rope_base) / half))
    cosine, sine = cos_sin(positions * inverse)
    signed = jnp.where(lane < half, -sine, sine)
    filled = positions - block_size * jnp.floor(positions * (1.0 / block_size))
    distance = filled - lane.astype(f32)
    live = distance > 0.0
    rates = [math.log1p(-(2.0 ** (-5 - h))) for h in range(head_count)]
    decay = [
        jnp.where(live, jnp.exp(jnp.maximum(distance, 0.0) * rate), 0.0) for rate in rates
    ]

    def rotated(raw):
        return raw * cosine + pltpu.roll(raw, half, 1) * signed

    get_q.wait()
    raw_query = mm(normal_in, wq[...])
    get_k.wait()
    raw_key = mm(normal_in, wk[...])
    queries, own = [], []
    for h in range(head_count):
        part = slice(h * key_size, (h + 1) * key_size)
        query = (rotated(raw_query[:, part]) * key_size ** (-0.5)).astype(bf16)
        key = rotated(raw_key[:, part]).astype(bf16)
        new_keys_ref[:, part] = key
        queries.append(query)
        weight = jnp.sum(query.astype(f32) * key.astype(f32), axis=1, keepdims=True)
        own.append(weight.astype(bf16).astype(f32))

    pl.semaphore_wait(barrier, len(peers))
    mine = extras.at[z, y, x]
    extra_z = [
        send(mine, mine, ez_s.at[o - 1], ez_r.at[o - 1], z_peers[o - 1]) for o in range(1, zs)
    ]

    rows = 2 * block_size
    for p in range(pairs):
        get_keys[p].wait()
        for h in range(head_count):
            stored = keys[2 * p : 2 * p + 2, :, h * key_size : (h + 1) * key_size]
            scores = mm_t(queries[h], stored.reshape(rows, key_size))
            for i in range(2):
                part = scores[:, i * block_size : (i + 1) * block_size] * decay[h]
                weights[h, :, p * rows + i * block_size : p * rows + (i + 1) * block_size] = (
                    jnp.where(row == 2 * p + i, part, 0.0).astype(bf16)
                )

    swaps = []
    for at, (copy, held) in enumerate(zip(get_ffn, (eg, eu, ed, dg, du, dd))):
        copy.wait()
        swaps.append(send(held.at[0], held.at[1], swap_s.at[at], swap_r.at[at], mate))
    for copy in extra_z:
        copy.wait_recv()
    column = extras.at[:, y, x]
    extra_plane = [
        send(column, column, ep_s.at[i], ep_r.at[i], plane_peers[i]) for i in range(len(around))
    ]

    get_v.wait()
    new_values = mm(normal_in, wv[...]).astype(bf16)
    new_values_ref[...] = new_values

    inside = [jnp.zeros((seq_count, value_size), f32) for _ in range(head_count)]
    carried = [jnp.zeros((seq_count, value_size), f32) for _ in range(head_count)]
    for p in range(pairs):
        get_values[p].wait()
        for h in range(head_count):
            stored = values[2 * p : 2 * p + 2, :, h * value_size : (h + 1) * value_size]
            inside[h] = inside[h] + mm(
                weights[h, :, p * rows : (p + 1) * rows], stored.reshape(rows, value_size)
            )
        get_state[p].wait()
        for h in range(head_count):
            chosen = jnp.concatenate(
                [jnp.where(row == 2 * p + i, queries[h].astype(f32), 0.0) for i in range(2)],
                axis=1,
            ).astype(bf16)
            held = state[2 * p : 2 * p + 2, h].reshape(2 * key_size, value_size)
            carried[h] = carried[h] + mm(chosen, held.astype(bf16))

    for h in range(head_count):
        part = slice(h * value_size, (h + 1) * value_size)
        fade = jnp.exp((filled[:, 0:1] + 1.0) * rates[h])
        retained = inside[h] + own[h] * new_values[:, part].astype(f32) + carried[h] * fade
        headed[:, part] = (retained * inverse_rms(retained)).astype(bf16)
    get_o.wait()
    mixer_out = mm(headed[...], wo[...])
    residual = widened + mixer_out * inverse_rms(mixer_out)
    normal_ffn = (residual * inverse_rms(residual) * ffn_ref[...]).astype(bf16)
    gathered[z, y, x] = normal_ffn

    block = gathered.at[z, y, x]
    from_z = [None] + [
        send(block, block, z_s.at[o - 1], z_r.at[o - 1], z_peers[o - 1]) for o in range(1, zs)
    ]

    def spread(o):
        if o:
            from_z[o].wait_recv()
        part = gathered.at[source(o), y, x]
        return [
            send(part, part, d_s.at[o, i], d_r.at[o, i], plane_peers[i])
            for i in range(len(around))
        ]

    from_plane = [spread(0)]

    for copy in get_shared:
        copy.wait()
    hidden = (silu(mm(normal_ffn, sg[...])) * mm(normal_ffn, su[...])).astype(bf16)
    combined = mm(hidden, sd[...])
    gate = 1.0 / (1.0 + jnp.exp(-dense_ref[...]))

    for o in range(1, zs):
        from_plane.append(spread(o))
    for copy in swaps + extra_plane:
        copy.wait_recv()

    def branches(o):
        at = source(o)
        for copy in from_plane[o]:
            copy.wait_recv()
        count = ys * xs * seq_count
        inputs = gathered[at].reshape(count, width)
        scale = extras[at].reshape(count, extras.shape[-1]).astype(f32)
        place = lax.broadcasted_iota(jnp.int32, scale.shape, 1)
        dense = (
            silu(mm_t(inputs, dg[...].reshape(-1, width)))
            * mm_t(inputs, du[...].reshape(-1, width))
        ).astype(bf16)
        terms = gate * mm(dense, dd[...].reshape(-1, width))
        for slot, expert in enumerate((me, mate)):
            chosen = (place == expert) | (place == expert + expert_count)
            weight = jnp.sum(jnp.where(chosen, scale, 0.0), axis=1, keepdims=True)
            inner = (silu(mm(inputs, eg[slot])) * mm(inputs, eu[slot])).astype(bf16)
            terms = terms + weight * mm(inner, ed[slot])
        partial[at] = terms.astype(bf16).reshape(partial.shape[1:])
        return [
            send(
                partial.at[at, beside(i)[0], beside(i)[1]],
                arrived.at[o, i],
                p_s.at[o, i],
                p_r.at[o, i],
                plane_peers[i],
            )
            for i in range(len(around))
        ]

    to_plane = [branches(o) for o in range(zs)]

    def plane_sum(o):
        for copy in to_plane[o]:
            copy.wait_recv()
        value = partial[source(o), y, x].astype(f32)
        for i in range(len(around)):
            value = value + arrived[o, i].astype(f32)
        return value

    combined = combined + plane_sum(0)
    to_home = []
    for o in range(1, zs):
        summed[o - 1] = plane_sum(o).astype(bf16)
        to_home.append(
            send(
                summed.at[o - 1],
                returned.at[o - 1],
                b_s.at[o - 1],
                b_r.at[o - 1],
                home_peers[o - 1],
            )
        )
    for o in range(1, zs):
        to_home[o - 1].wait_recv()
        combined = combined + returned[o - 1].astype(f32)
    out_ref[...] = (residual + combined * inverse_rms(combined)).astype(bf16)
    for copy in started:
        copy.wait_send()


def finish(a_ref, b_ref, c_ref, a_out, b_out, c_out, sems):
    copies = [
        pltpu.make_async_copy(origin, place, sems.at[at])
        for at, (origin, place) in enumerate([(a_ref, a_out), (b_ref, b_out), (c_ref, c_out)])
    ]
    for copy in copies:
        copy.start()
    for copy in copies:
        copy.wait()


def whole_layer(vectors, streams, shapes, dims, expert_count):
    seq_count, width, head_count, top_k = shapes
    zs, ys, xs = dims
    wq, wk, wv, wo, keys, values, state = streams[:7]
    experts, dense, shared = streams[7:10], streams[10:13], streams[13:16]
    z1, others = max(zs - 1, 1), max(ys * xs - 1, 1)
    extra = 2 * expert_count
    extra += -extra % lanes
    dma = pltpu.SemaphoreType.DMA
    vmem = pl.BlockSpec(memory_space=pltpu.VMEM)
    anywhere = pl.BlockSpec(memory_space=pl.ANY)
    grid = (zs, ys, xs, seq_count)
    scratch = [pltpu.VMEM(w.shape, w.dtype) for w in streams[:7]]
    scratch += [pltpu.VMEM((2,) + w.shape[1:], bf16) for w in experts]
    scratch += [pltpu.VMEM((2,) + w.shape, bf16) for w in dense]
    scratch += [pltpu.VMEM(w.shape, bf16) for w in shared]
    scratch += [
        pltpu.VMEM((head_count, seq_count, seq_count * keys.shape[1]), bf16),
        pltpu.VMEM((seq_count, values.shape[2]), bf16),
        pltpu.VMEM((3, 8, lanes), f32),
        pltpu.VMEM(grid + (extra,), bf16),
        pltpu.VMEM(grid + (width,), bf16),
        pltpu.VMEM(grid + (width,), bf16),
        pltpu.VMEM((zs, others, seq_count, width), bf16),
        pltpu.VMEM((z1, seq_count, width), bf16),
        pltpu.VMEM((z1, seq_count, width), bf16),
    ]
    pairs = (seq_count // 2,)
    sems = [(4,), pairs, pairs, pairs, (9,), (6,), (6,), (z1,), (z1,), (others,), (others,)]
    sems += [(z1,), (z1,)] + [(zs, others)] * 4 + [(z1,), (z1,)]
    out_shapes = [(seq_count, width), (seq_count, keys.shape[2]), (seq_count, values.shape[2])]
    results = pl.pallas_call(
        functools.partial(layer, dims, head_count, expert_count),
        out_shape=[pltpu.VMEM(shape, bf16) for shape in out_shapes],
        in_specs=[vmem] * len(vectors) + [anywhere] * len(streams),
        out_specs=[vmem] * 3,
        scratch_shapes=scratch + [dma(shape) for shape in sems],
        compiler_params=pltpu.CompilerParams(
            collective_id=0, has_side_effects=True, vmem_limit_bytes=58 * 1024 * 1024
        ),
    )(*vectors, *streams)
    return pl.pallas_call(
        finish,
        out_shape=[jax.ShapeDtypeStruct(shape, bf16) for shape in out_shapes],
        in_specs=[vmem] * 3,
        out_specs=[anywhere] * 3,
        scratch_shapes=[dma((3,))],
        compiler_params=pltpu.CompilerParams(vmem_limit_bytes=1024 * 1024),
    )(*results)


def per_device(
    tokens,
    lengths,
    cache_keys,
    cache_values,
    retention_state,
    mix_gain,
    query_weight,
    key_weight,
    value_weight,
    out_weight,
    ffn_gain,
    routes,
    route_scores,
    expert_gate,
    expert_up,
    expert_down,
    shared_gate,
    shared_up,
    shared_down,
    dense_gate,
    dense_up,
    dense_down,
    dense_mix,
):
    device_count = lax.axis_size("ep")
    expert_count = device_count * expert_gate.shape[0]
    seq_count, width = tokens.shape
    vectors = (
        tokens,
        lengths.reshape(1, seq_count),
        routes.T,
        route_scores.T,
        mix_gain.reshape(1, width),
        ffn_gain.reshape(1, width),
        dense_mix.reshape(1, width),
    )
    streams = (
        query_weight,
        key_weight,
        value_weight,
        out_weight,
        cache_keys,
        cache_values,
        retention_state,
        expert_gate,
        expert_up,
        expert_down,
        dense_gate,
        dense_up,
        dense_down,
        shared_gate,
        shared_up,
        shared_down,
    )
    shapes = (seq_count, width, retention_state.shape[1], routes.shape[1])
    return tuple(
        whole_layer(vectors, streams, shapes, slice_dims(device_count), expert_count)
    )


def solution(mesh):
    in_specs = (
        P("ep", None),
        P("ep"),
        P("ep", None, None),
        P("ep", None, None),
        P("ep", None, None, None),
        P(),
        P(),
        P(),
        P(),
        P(),
        P(),
        P("ep", None),
        P("ep", None),
        P("ep", None, None),
        P("ep", None, None),
        P("ep", None, None),
        P(),
        P(),
        P(),
        P("ep", None),
        P("ep", None),
        P("ep", None),
        P(),
    )
    out_specs = (P("ep", None), P("ep", None), P("ep", None))
    return jax.shard_map(
        per_device, mesh=mesh, in_specs=in_specs, out_specs=out_specs, check_vma=False
    )
```

time: 47.9 us -> 36.8 us (0.77)
  Pallas kernels: 45.6 us -> 36 us
  local copies, waits for them, and re-layouts: 1.38 us -> 0 us
    pallas_call x2, Pallas kernels: 45.6 us -> 36 us  [the longest x1 35.3 us: whole_layer(): pl.pallas_call(functools.partial(layer, dims, head_count, expert_count),...]
    unnamed x1 -> x0, local copies, waits for them, and re-layouts: 1.38 us -> none
where the time goes in v2:
time: 36.8 us; the launch traced here: 36.6 us
  Pallas kernels  36 us (98%)
  between operations  0.65 us (2%)
    pallas_call x1, Pallas kernels, whole_layer(): pl.pallas_call(functools.partial(layer, dims, head_count, expert_count),...  35.3 us

profile of v2, /device:TPU:0, one launch (start us, length us, event | category | flops | bytes accessed | tf_op | source)
XLA Modules:
  0.0 36.6 jit_solution(15338840733812714979)
XLA Ops:
  0.6 35.3 %shard_map.238 = (bf16[16,1024]{1,0:T(8,128)(2,1)S(1)}, bf16[16,512]{1,0:T(8,128)(2,1)S(1)}, bf16[16,1024]{1,0:T(8,128)(2,1)S(1)}) custom-call(bf16[16,1024]{1,0:T(8,128)(2,1)} %tokens_ref.1, s32[1,16]{1,0:T(1,128)} %bitcast.11, s32[6,16]{1,0:T(8,128)} %bitcast.6, f32[6,16]{1,0:T(8,128)} %bitcast.7, f32[1,1024]{1,0:T(1,128)} %bitcast.8, f32[1,1024]{1,0:T(1,128)} %bitcast.9, ...), custom_call_target="tpu_custom_call" | custom-call | tf_op jit(solution)/shard_map/pallas_call | solution.py:504
  36.0 0.7 %shard_map.239 = (bf16[16,1024]{1,0:T(8,128)(2,1)}, bf16[16,512]{1,0:T(8,128)(2,1)}, bf16[16,1024]{1,0:T(8,128)(2,1)}) custom-call(bf16[16,1024]{1,0:T(8,128)(2,1)S(1)} %get-tuple-element.6.a_ref, bf16[16,512]{1,0:T(8,128)(2,1)S(1)} %get-tuple-element.7.b_ref, bf16[16,1024]{1,0:T(8,128)(2,1)S(1)} %get-tuple-element.8.c_ref), custom_call_target="tpu_custom_call" | custom-call | tf_op jit(solution)/shard_map/pallas_call | solution.py:514

commit v3 on v2

--- a/solution.py
+++ b/solution.py
@@ -75,26 +75,17 @@
     return device_count // (2 * side * side), side, side
 
 
-def crossed(at, by):
-    moved, bit = at, 1
-    while bit <= by:
-        if by & bit:
-            moved = moved + bit - 2 * bit * lax.rem(at // bit, 2)
-        bit *= 2
-    return moved
-
-
 def layer(
     dims,
     head_count,
     expert_count,
-    tokens_ref,
-    lengths_ref,
-    routes_ref,
-    scores_ref,
-    mix_ref,
-    ffn_ref,
-    dense_ref,
+    tokens_hbm,
+    lengths_hbm,
+    routes_hbm,
+    scores_hbm,
+    mix_hbm,
+    ffn_hbm,
+    dense_hbm,
     wq_hbm,
     wk_hbm,
     wv_hbm,
@@ -114,6 +105,13 @@
     out_ref,
     new_keys_ref,
     new_values_ref,
+    tokens_ref,
+    lengths_ref,
+    routes_ref,
+    scores_ref,
+    mix_ref,
+    ffn_ref,
+    dense_ref,
     wq,
     wk,
     wv,
@@ -131,7 +129,6 @@
     su,
     sd,
     weights,
-    headed,
     small,
     extras,
     gathered,
@@ -139,11 +136,7 @@
     arrived,
     summed,
     returned,
-    w_sem,
-    k_sem,
-    v_sem,
-    s_sem,
-    f_sem,
+    l_sem,
     swap_s,
     swap_r,
     ez_s,
@@ -172,68 +165,78 @@
     x = lax.rem(me // 2, xs)
     y = lax.rem(me // (2 * xs), ys)
     z = me // (2 * xs * ys)
-    paired = zs & (zs - 1) == 0
 
     def device(zz, yy, xx, cc):
         return ((zz * ys + yy) * xs + xx) * 2 + cc
 
-    def source(o):
-        return crossed(z, o) if paired else lax.rem(z - o + zs, zs)
-
-    def target(o):
-        return crossed(z, o) if paired else lax.rem(z + o, zs)
-
-    around = [(dy, dx) for dy in range(ys) for dx in range(xs) if dy or dx]
+    planes = [k + (k - z + zs) // zs for k in range(zs - 1)]
+    around = sorted(
+        ((dy, dx) for dy in range(ys) for dx in range(xs) if dy or dx),
+        key=lambda step: -min(step[0], ys - step[0]) - min(step[1], xs - step[1]),
+    )
 
     def beside(i):
         dy, dx = around[i]
         return lax.rem(y + dy, ys), lax.rem(x + dx, xs)
 
+    def behind(i):
+        dy, dx = around[i]
+        return lax.rem(y - dy + ys, ys), lax.rem(x - dx + xs, xs)
+
     mate = device(z, y, x, 1 - core)
-    z_peers = [device(target(o), y, x, core) for o in range(1, zs)]
-    home_peers = [device(source(o), y, x, core) for o in range(1, zs)]
+    z_peers = [device(plane, y, x, core) for plane in planes]
     plane_peers = [device(z, *beside(i), core) for i in range(len(around))]
 
-    def load(origin, place, sem):
-        copy = pltpu.make_async_copy(origin, place, sem)
-        copy.start()
-        return copy
-
-    get_q = load(wq_hbm, wq, w_sem.at[0])
-    get_k = load(wk_hbm, wk, w_sem.at[1])
-    get_keys = [
-        load(keys_hbm.at[pl.ds(2 * p, 2)], keys.at[pl.ds(2 * p, 2)], k_sem.at[p])
-        for p in range(pairs)
-    ]
-    get_ffn = [
-        load(origin, place, f_sem.at[at])
-        for at, (origin, place) in enumerate(
-            [
-                (eg_hbm, eg.at[pl.ds(0, 1)]),
-                (eu_hbm, eu.at[pl.ds(0, 1)]),
-                (ed_hbm, ed.at[pl.ds(0, 1)]),
-                (dg_hbm, dg.at[0]),
-                (du_hbm, du.at[0]),
-                (dd_hbm, dd.at[0]),
-            ]
-        )
-    ]
-    get_v = load(wv_hbm, wv, w_sem.at[2])
-    get_values, get_state = [], []
+    waiting = []
+
+    def plan(name, origin, place, pieces=1):
+        count = origin.shape[0] // pieces
+        for at in range(pieces):
+            part = pl.ds(at * count, count)
+            index = len(waiting)
+            copy = pltpu.make_async_copy(origin.at[part], place.at[part], l_sem.at[index])
+            waiting.append((name, copy))
+
+    plan("tokens", tokens_hbm, tokens_ref)
+    plan("tokens", mix_hbm, mix_ref)
+    plan("query", wq_hbm, wq, 2)
+    plan("small", lengths_hbm, lengths_ref)
+    plan("small", routes_hbm, routes_ref)
+    plan("small", scores_hbm, scores_ref)
+    plan("key", wk_hbm, wk, 2)
+    for p in range(0, pairs, 2):
+        part = pl.ds(2 * p, 4)
+        plan(("keys", p), keys_hbm.at[part], keys.at[part])
+    plan("value", wv_hbm, wv, 4)
     for p in range(pairs):
         part = pl.ds(2 * p, 2)
-        get_values.append(load(values_hbm.at[part], values.at[part], v_sem.at[p]))
-        get_state.append(load(state_hbm.at[part], state.at[part], s_sem.at[p]))
-    get_o = load(wo_hbm, wo, w_sem.at[3])
-    get_shared = [
-        load(origin, place, f_sem.at[6 + at])
-        for at, (origin, place) in enumerate([(sg_hbm, sg), (su_hbm, su), (sd_hbm, sd)])
-    ]
+        plan(("values", p), values_hbm.at[part], values.at[part])
+        plan(("state", p), state_hbm.at[part], state.at[part], 2)
+        if p == 0:
+            plan("swap", eg_hbm, eg.at[pl.ds(0, 1)])
+            plan("swap", eu_hbm, eu.at[pl.ds(0, 1)])
+            plan("swap", ed_hbm, ed.at[pl.ds(0, 1)])
+            plan("swap", dg_hbm, dg.at[0])
+            plan("swap", du_hbm, du.at[0])
+            plan("swap", dd_hbm, dd.at[0])
+        if p == pairs // 2 - 1:
+            plan("out", wo_hbm, wo, 4)
+            plan("out", ffn_hbm, ffn_ref)
+    plan("shared", sg_hbm, sg)
+    plan("shared", su_hbm, su)
+    plan("shared", sd_hbm, sd)
+    plan("shared", dense_hbm, dense_ref)
+
+    for _, copy in waiting:
+        copy.start()
+
+    def need(name):
+        for label, copy in waiting:
+            if label == name:
+                copy.wait()
 
     barrier = pltpu.get_barrier_semaphore()
     peers = z_peers + plane_peers + [mate]
-    if not paired:
-        peers = peers + home_peers
     for peer in peers:
         pl.semaphore_signal(
             barrier, inc=1, device_id=(peer,), device_id_type=pl.DeviceIdType.MESH
@@ -252,11 +255,22 @@
         )
         copy.start()
         started.append(copy)
-        return copy
-
+
+    def landed(place, sem):
+        pltpu.make_async_remote_copy(
+            src_ref=place,
+            dst_ref=place,
+            send_sem=sem,
+            recv_sem=sem,
+            device_id=(mate,),
+            device_id_type=pl.DeviceIdType.MESH,
+        ).wait_recv()
+
+    need("tokens")
     widened = tokens_ref[...].astype(f32)
     normal_in = (widened * inverse_rms(widened) * mix_ref[...]).astype(bf16)
 
+    need("small")
     top_k = routes_ref.shape[0]
     small[...] = jnp.zeros_like(small)
     small[0, 0:1, 0:seq_count] = lengths_ref[...].astype(f32)
@@ -295,9 +309,9 @@
     def rotated(raw):
         return raw * cosine + pltpu.roll(raw, half, 1) * signed
 
-    get_q.wait()
+    need("query")
     raw_query = mm(normal_in, wq[...])
-    get_k.wait()
+    need("key")
     raw_key = mm(normal_in, wk[...])
     queries, own = [], []
     for h in range(head_count):
@@ -311,13 +325,13 @@
 
     pl.semaphore_wait(barrier, len(peers))
     mine = extras.at[z, y, x]
-    extra_z = [
-        send(mine, mine, ez_s.at[o - 1], ez_r.at[o - 1], z_peers[o - 1]) for o in range(1, zs)
-    ]
+    for k, peer in enumerate(z_peers):
+        send(mine, mine, ez_s.at[k], ez_r.at[z], peer)
 
     rows = 2 * block_size
     for p in range(pairs):
-        get_keys[p].wait()
+        if p % 2 == 0:
+            need(("keys", p))
         for h in range(head_count):
             stored = keys[2 * p : 2 * p + 2, :, h * key_size : (h + 1) * key_size]
             scores = mm_t(queries[h], stored.reshape(rows, key_size))
@@ -327,31 +341,33 @@
                     jnp.where(row == 2 * p + i, part, 0.0).astype(bf16)
                 )
 
-    swaps = []
-    for at, (copy, held) in enumerate(zip(get_ffn, (eg, eu, ed, dg, du, dd))):
-        copy.wait()
-        swaps.append(send(held.at[0], held.at[1], swap_s.at[at], swap_r.at[at], mate))
-    for copy in extra_z:
-        copy.wait_recv()
-    column = extras.at[:, y, x]
-    extra_plane = [
-        send(column, column, ep_s.at[i], ep_r.at[i], plane_peers[i]) for i in range(len(around))
-    ]
-
-    get_v.wait()
+    need("value")
     new_values = mm(normal_in, wv[...]).astype(bf16)
     new_values_ref[...] = new_values
 
+    wide_values = new_values.astype(f32)
     inside = [jnp.zeros((seq_count, value_size), f32) for _ in range(head_count)]
     carried = [jnp.zeros((seq_count, value_size), f32) for _ in range(head_count)]
+    fades = [jnp.exp((filled[:, 0:1] + 1.0) * rate) for rate in rates]
+    residuals = []
+    part_rows = seq_count // 2
+
+    def piece(at, q):
+        return gathered.at[at, y, x, pl.ds(q * part_rows, part_rows)]
+
+    def spread(q, at):
+        part = piece(at, q)
+        for i, peer in enumerate(plane_peers):
+            send(part, part, d_s.at[q, at, i], d_r.at[q, at, i], peer)
+
     for p in range(pairs):
-        get_values[p].wait()
+        need(("values", p))
         for h in range(head_count):
             stored = values[2 * p : 2 * p + 2, :, h * value_size : (h + 1) * value_size]
             inside[h] = inside[h] + mm(
                 weights[h, :, p * rows : (p + 1) * rows], stored.reshape(rows, value_size)
             )
-        get_state[p].wait()
+        need(("state", p))
         for h in range(head_count):
             chosen = jnp.concatenate(
                 [jnp.where(row == 2 * p + i, queries[h].astype(f32), 0.0) for i in range(2)],
@@ -359,49 +375,61 @@
             ).astype(bf16)
             held = state[2 * p : 2 * p + 2, h].reshape(2 * key_size, value_size)
             carried[h] = carried[h] + mm(chosen, held.astype(bf16))
-
-    for h in range(head_count):
-        part = slice(h * value_size, (h + 1) * value_size)
-        fade = jnp.exp((filled[:, 0:1] + 1.0) * rates[h])
-        retained = inside[h] + own[h] * new_values[:, part].astype(f32) + carried[h] * fade
-        headed[:, part] = (retained * inverse_rms(retained)).astype(bf16)
-    get_o.wait()
-    mixer_out = mm(headed[...], wo[...])
-    residual = widened + mixer_out * inverse_rms(mixer_out)
-    normal_ffn = (residual * inverse_rms(residual) * ffn_ref[...]).astype(bf16)
-    gathered[z, y, x] = normal_ffn
-
-    block = gathered.at[z, y, x]
-    from_z = [None] + [
-        send(block, block, z_s.at[o - 1], z_r.at[o - 1], z_peers[o - 1]) for o in range(1, zs)
-    ]
-
-    def spread(o):
-        if o:
-            from_z[o].wait_recv()
-        part = gathered.at[source(o), y, x]
-        return [
-            send(part, part, d_s.at[o, i], d_r.at[o, i], plane_peers[i])
-            for i in range(len(around))
-        ]
-
-    from_plane = [spread(0)]
-
-    for copy in get_shared:
-        copy.wait()
+        if p == 1:
+            need("swap")
+            for at, held in enumerate((eg, eu, ed, dg, du, dd)):
+                send(held.at[0], held.at[1], swap_s.at[at], swap_r.at[at], mate)
+        if p == pairs // 2:
+            for plane in planes:
+                landed(extras.at[plane, y, x], ez_r.at[plane])
+            column = extras.at[:, y, x]
+            for i, peer in enumerate(plane_peers):
+                send(column, column, ep_s.at[i], ep_r.at[i], peer)
+        if (p + 1) % (pairs // 2):
+            continue
+        q = p // (pairs // 2)
+        cut = slice(q * part_rows, (q + 1) * part_rows)
+        heads = []
+        for h in range(head_count):
+            part = slice(h * value_size, (h + 1) * value_size)
+            retained = (
+                inside[h][cut]
+                + own[h][cut] * wide_values[cut, part]
+                + carried[h][cut] * fades[h][cut]
+            )
+            heads.append(retained * inverse_rms(retained))
+        if q == 0:
+            need("out")
+        mixer_out = mm(jnp.concatenate(heads, axis=1).astype(bf16), wo[...])
+        residual = widened[cut] + mixer_out * inverse_rms(mixer_out)
+        residuals.append(residual)
+        gathered[z, y, x, cut] = (residual * inverse_rms(residual) * ffn_ref[...]).astype(bf16)
+        block = piece(z, q)
+        for k, peer in enumerate(z_peers):
+            send(block, block, z_s.at[q, k], z_r.at[q, z], peer)
+        spread(q, z)
+
+    residual = jnp.concatenate(residuals, axis=0)
+    normal_ffn = gathered[z, y, x]
+    need("shared")
     hidden = (silu(mm(normal_ffn, sg[...])) * mm(normal_ffn, su[...])).astype(bf16)
     combined = mm(hidden, sd[...])
     gate = 1.0 / (1.0 + jnp.exp(-dense_ref[...]))
 
-    for o in range(1, zs):
-        from_plane.append(spread(o))
-    for copy in swaps + extra_plane:
-        copy.wait_recv()
-
-    def branches(o):
-        at = source(o)
-        for copy in from_plane[o]:
-            copy.wait_recv()
+    for plane in planes:
+        for q in range(2):
+            landed(piece(plane, q), z_r.at[q, plane])
+            spread(q, plane)
+    for at, held in enumerate((eg, eu, ed, dg, du, dd)):
+        landed(held.at[1], swap_r.at[at])
+    for i in range(len(around)):
+        landed(extras.at[:, behind(i)[0], behind(i)[1]], ep_r.at[i])
+
+    def branches(at):
+        for q in range(2):
+            for i in range(len(around)):
+                part = pl.ds(q * part_rows, part_rows)
+                landed(gathered.at[at, behind(i)[0], behind(i)[1], part], d_r.at[q, at, i])
         count = ys * xs * seq_count
         inputs = gathered[at].reshape(count, width)
         scale = extras[at].reshape(count, extras.shape[-1]).astype(f32)
@@ -417,43 +445,36 @@
             inner = (silu(mm(inputs, eg[slot])) * mm(inputs, eu[slot])).astype(bf16)
             terms = terms + weight * mm(inner, ed[slot])
         partial[at] = terms.astype(bf16).reshape(partial.shape[1:])
-        return [
+        for i, peer in enumerate(plane_peers):
             send(
                 partial.at[at, beside(i)[0], beside(i)[1]],
-                arrived.at[o, i],
-                p_s.at[o, i],
-                p_r.at[o, i],
-                plane_peers[i],
+                arrived.at[at, i],
+                p_s.at[at, i],
+                p_r.at[at, i],
+                peer,
             )
-            for i in range(len(around))
-        ]
-
-    to_plane = [branches(o) for o in range(zs)]
-
-    def plane_sum(o):
-        for copy in to_plane[o]:
-            copy.wait_recv()
-        value = partial[source(o), y, x].astype(f32)
+
+    for at in range(zs):
+        branches(at)
+
+    def plane_sum(at):
         for i in range(len(around)):
-            value = value + arrived[o, i].astype(f32)
+            landed(arrived.at[at, i], p_r.at[at, i])
+        value = partial[at, y, x].astype(f32)
+        for i in range(len(around)):
+            value = value + arrived[at, i].astype(f32)
         return value
 
-    combined = combined + plane_sum(0)
-    to_home = []
-    for o in range(1, zs):
-        summed[o - 1] = plane_sum(o).astype(bf16)
-        to_home.append(
-            send(
-                summed.at[o - 1],
-                returned.at[o - 1],
-                b_s.at[o - 1],
-                b_r.at[o - 1],
-                home_peers[o - 1],
-            )
-        )
-    for o in range(1, zs):
-        to_home[o - 1].wait_recv()
-        combined = combined + returned[o - 1].astype(f32)
+    for k, peer in enumerate(z_peers):
+        if k == zs - 2:
+            combined = combined + plane_sum(z)
+        summed[k] = plane_sum(planes[k]).astype(bf16)
+        send(summed.at[k], returned.at[z], b_s.at[k], b_r.at[z], peer)
+    if zs == 1:
+        combined = combined + plane_sum(z)
+    for plane in reversed(planes):
+        landed(returned.at[plane], b_r.at[plane])
+        combined = combined + returned[plane].astype(f32)
     out_ref[...] = (residual + combined * inverse_rms(combined)).astype(bf16)
     for copy in started:
         copy.wait_send()
@@ -482,29 +503,28 @@
     vmem = pl.BlockSpec(memory_space=pltpu.VMEM)
     anywhere = pl.BlockSpec(memory_space=pl.ANY)
     grid = (zs, ys, xs, seq_count)
-    scratch = [pltpu.VMEM(w.shape, w.dtype) for w in streams[:7]]
+    scratch = [pltpu.VMEM(w.shape, w.dtype) for w in vectors + streams[:7]]
     scratch += [pltpu.VMEM((2,) + w.shape[1:], bf16) for w in experts]
     scratch += [pltpu.VMEM((2,) + w.shape, bf16) for w in dense]
     scratch += [pltpu.VMEM(w.shape, bf16) for w in shared]
     scratch += [
         pltpu.VMEM((head_count, seq_count, seq_count * keys.shape[1]), bf16),
-        pltpu.VMEM((seq_count, values.shape[2]), bf16),
         pltpu.VMEM((3, 8, lanes), f32),
         pltpu.VMEM(grid + (extra,), bf16),
         pltpu.VMEM(grid + (width,), bf16),
         pltpu.VMEM(grid + (width,), bf16),
         pltpu.VMEM((zs, others, seq_count, width), bf16),
         pltpu.VMEM((z1, seq_count, width), bf16),
-        pltpu.VMEM((z1, seq_count, width), bf16),
+        pltpu.VMEM((zs, seq_count, width), bf16),
     ]
-    pairs = (seq_count // 2,)
-    sems = [(4,), pairs, pairs, pairs, (9,), (6,), (6,), (z1,), (z1,), (others,), (others,)]
-    sems += [(z1,), (z1,)] + [(zs, others)] * 4 + [(z1,), (z1,)]
+    sems = [(9 * seq_count,), (6,), (6,)]
+    sems += [(z1,), (zs,), (others,), (others,), (2, z1), (2, zs)]
+    sems += [(2, zs, others)] * 2 + [(zs, others)] * 2 + [(z1,), (zs,)]
     out_shapes = [(seq_count, width), (seq_count, keys.shape[2]), (seq_count, values.shape[2])]
     results = pl.pallas_call(
         functools.partial(layer, dims, head_count, expert_count),
         out_shape=[pltpu.VMEM(shape, bf16) for shape in out_shapes],
-        in_specs=[vmem] * len(vectors) + [anywhere] * len(streams),
+        in_specs=[anywhere] * (len(vectors) + len(streams)),
         out_specs=[vmem] * 3,
         scratch_shapes=scratch + [dma(shape) for shape in sems],
         compiler_params=pltpu.CompilerParams(

time: 36.8 us -> 31.9 us (0.87)
  Pallas kernels: 36 us -> 31.1 us
    pallas_call x1, Pallas kernels: 35.3 us -> 30.5 us  [whole_layer(): pl.pallas_call(functools.partial(layer, dims, head_count, expert_count),...]
where the time goes in v3:
time: 31.9 us; the launch traced here: 31.8 us
  Pallas kernels  31.1 us (97%)
  between operations  0.65 us (2%)
    pallas_call x1, Pallas kernels, whole_layer(): pl.pallas_call(functools.partial(layer, dims, head_count, expert_count),...  30.5 us
    pallas_call x1, Pallas kernels, whole_layer(): pl.pallas_call(finish, out_shape=[jax.ShapeDtypeStruct(shape, bf16) for s...  0.66 us

profile of v3, /device:TPU:0, one launch (start us, length us, event | category | flops | bytes accessed | tf_op | source)
XLA Modules:
  0.0 31.8 jit_solution(9808113804752426263)
XLA Ops:
  0.6 30.5 %shard_map.238 = (bf16[16,1024]{1,0:T(8,128)(2,1)S(1)}, bf16[16,512]{1,0:T(8,128)(2,1)S(1)}, bf16[16,1024]{1,0:T(8,128)(2,1)S(1)}) custom-call(bf16[16,1024]{1,0:T(8,128)(2,1)} %tokens_hbm.1, s32[1,16]{1,0:T(1,128)} %bitcast.11, s32[6,16]{1,0:T(8,128)} %bitcast.6, f32[6,16]{1,0:T(8,128)} %bitcast.7, f32[1,1024]{1,0:T(1,128)} %bitcast.8, f32[1,1024]{1,0:T(1,128)} %bitcast.9, ...), custom_call_target="tpu_custom_call" | custom-call | tf_op jit(solution)/shard_map/pallas_call | solution.py:524
  31.1 0.7 %shard_map.239 = (bf16[16,1024]{1,0:T(8,128)(2,1)}, bf16[16,512]{1,0:T(8,128)(2,1)}, bf16[16,1024]{1,0:T(8,128)(2,1)}) custom-call(bf16[16,1024]{1,0:T(8,128)(2,1)S(1)} %get-tuple-element.6.a_ref, bf16[16,512]{1,0:T(8,128)(2,1)S(1)} %get-tuple-element.7.b_ref, bf16[16,1024]{1,0:T(8,128)(2,1)S(1)} %get-tuple-element.8.c_ref), custom_call_target="tpu_custom_call" | custom-call | tf_op jit(solution)/shard_map/pallas_call | solution.py:534

commit v4 on v3

--- a/solution.py
+++ b/solution.py
@@ -136,6 +136,7 @@
     arrived,
     summed,
     returned,
+    total,
     l_sem,
     swap_s,
     swap_r,
@@ -184,6 +185,17 @@
         return lax.rem(y - dy + ys, ys), lax.rem(x - dx + xs, xs)
 
     mate = device(z, y, x, 1 - core)
+    direct = zs > 2
+    last = zs - 1
+    far = last - z
+    at_end = (z == 0) | (z == last)
+
+    def unless(condition, action):
+        if direct:
+            pl.when(jnp.logical_not(condition))(action)
+        else:
+            action()
+
     z_peers = [device(plane, y, x, core) for plane in planes]
     plane_peers = [device(z, *beside(i), core) for i in range(len(around))]
 
@@ -227,8 +239,20 @@
     plan("shared", sd_hbm, sd)
     plan("shared", dense_hbm, dense_ref)
 
-    for _, copy in waiting:
-        copy.start()
+    def swap_loads():
+        for label, copy in waiting:
+            if label == "swap":
+                copy.start()
+
+    before = None
+    for label, copy in waiting:
+        if label == "swap" and before != "swap":
+            pl.when(core == 1)(swap_loads)
+        if label == "shared" and before != "shared":
+            pl.when(core == 0)(swap_loads)
+        before = label
+        if label != "swap":
+            copy.start()
 
     def need(name):
         for label, copy in waiting:
@@ -237,12 +261,33 @@
 
     barrier = pltpu.get_barrier_semaphore()
     peers = z_peers + plane_peers + [mate]
+    peers += [device(plane, *beside(i), core) for plane in planes for i in range(len(around))]
     for peer in peers:
         pl.semaphore_signal(
             barrier, inc=1, device_id=(peer,), device_id_type=pl.DeviceIdType.MESH
         )
 
     started = []
+
+    def drained(place, sem):
+        pltpu.make_async_remote_copy(
+            src_ref=place,
+            dst_ref=place,
+            send_sem=sem,
+            recv_sem=sem,
+            device_id=(mate,),
+            device_id_type=pl.DeviceIdType.MESH,
+        ).wait_send()
+
+    def launch(origin, place, send_sem, recv_sem, peer):
+        pltpu.make_async_remote_copy(
+            src_ref=origin,
+            dst_ref=place,
+            send_sem=send_sem,
+            recv_sem=recv_sem,
+            device_id=(peer,),
+            device_id_type=pl.DeviceIdType.MESH,
+        ).start()
 
     def send(origin, place, send_sem, recv_sem, peer):
         copy = pltpu.make_async_remote_copy(
@@ -323,10 +368,6 @@
         weight = jnp.sum(query.astype(f32) * key.astype(f32), axis=1, keepdims=True)
         own.append(weight.astype(bf16).astype(f32))
 
-    pl.semaphore_wait(barrier, len(peers))
-    mine = extras.at[z, y, x]
-    for k, peer in enumerate(z_peers):
-        send(mine, mine, ez_s.at[k], ez_r.at[z], peer)
 
     rows = 2 * block_size
     for p in range(pairs):
@@ -350,6 +391,25 @@
     carried = [jnp.zeros((seq_count, value_size), f32) for _ in range(head_count)]
     fades = [jnp.exp((filled[:, 0:1] + 1.0) * rate) for rate in rates]
     residuals = []
+
+    def swap_copies():
+        return [
+            pltpu.make_async_remote_copy(
+                src_ref=held.at[0],
+                dst_ref=held.at[1],
+                send_sem=swap_s.at[at],
+                recv_sem=swap_r.at[at],
+                device_id=(mate,),
+                device_id_type=pl.DeviceIdType.MESH,
+            )
+            for at, held in enumerate((eg, eu, ed, dg, du, dd))
+        ]
+
+    def swap_weights():
+        need("swap")
+        for copy in swap_copies():
+            copy.start()
+
     part_rows = seq_count // 2
 
     def piece(at, q):
@@ -358,7 +418,7 @@
     def spread(q, at):
         part = piece(at, q)
         for i, peer in enumerate(plane_peers):
-            send(part, part, d_s.at[q, at, i], d_r.at[q, at, i], peer)
+            launch(part, part, d_s.at[q, at, i], d_r.at[q, at, i], peer)
 
     for p in range(pairs):
         need(("values", p))
@@ -376,15 +436,11 @@
             held = state[2 * p : 2 * p + 2, h].reshape(2 * key_size, value_size)
             carried[h] = carried[h] + mm(chosen, held.astype(bf16))
         if p == 1:
-            need("swap")
-            for at, held in enumerate((eg, eu, ed, dg, du, dd)):
-                send(held.at[0], held.at[1], swap_s.at[at], swap_r.at[at], mate)
-        if p == pairs // 2:
-            for plane in planes:
-                landed(extras.at[plane, y, x], ez_r.at[plane])
-            column = extras.at[:, y, x]
-            for i, peer in enumerate(plane_peers):
-                send(column, column, ep_s.at[i], ep_r.at[i], peer)
+            pl.semaphore_wait(barrier, len(peers))
+            mine = extras.at[z, y, x]
+            for k, peer in enumerate(z_peers):
+                send(mine, mine, ez_s.at[k], ez_r.at[z], peer)
+            pl.when(core == 1)(swap_weights)
         if (p + 1) % (pairs // 2):
             continue
         q = p // (pairs // 2)
@@ -409,17 +465,32 @@
             send(block, block, z_s.at[q, k], z_r.at[q, z], peer)
         spread(q, z)
 
+    pl.when(core == 0)(swap_weights)
+    for plane in planes:
+        landed(extras.at[plane, y, x], ez_r.at[plane])
+    column = extras.at[:, y, x]
+    for i, peer in enumerate(plane_peers):
+        send(column, column, ep_s.at[i], ep_r.at[i], peer)
     residual = jnp.concatenate(residuals, axis=0)
     normal_ffn = gathered[z, y, x]
+    def forward(k):
+        def onward():
+            for q in range(2):
+                landed(piece(planes[k], q), z_r.at[q, planes[k]])
+                spread(q, planes[k])
+
+        onward()
+
+    for k in range(0, max(zs - 2, min(1, zs - 1))):
+        forward(k)
     need("shared")
     hidden = (silu(mm(normal_ffn, sg[...])) * mm(normal_ffn, su[...])).astype(bf16)
     combined = mm(hidden, sd[...])
     gate = 1.0 / (1.0 + jnp.exp(-dense_ref[...]))
 
-    for plane in planes:
-        for q in range(2):
-            landed(piece(plane, q), z_r.at[q, plane])
-            spread(q, plane)
+    if zs > 2:
+        forward(zs - 2)
+
     for at, held in enumerate((eg, eu, ed, dg, du, dd)):
         landed(held.at[1], swap_r.at[at])
     for i in range(len(around)):
@@ -445,14 +516,39 @@
             inner = (silu(mm(inputs, eg[slot])) * mm(inputs, eu[slot])).astype(bf16)
             terms = terms + weight * mm(inner, ed[slot])
         partial[at] = terms.astype(bf16).reshape(partial.shape[1:])
-        for i, peer in enumerate(plane_peers):
-            send(
-                partial.at[at, beside(i)[0], beside(i)[1]],
-                arrived.at[at, i],
-                p_s.at[at, i],
-                p_r.at[at, i],
-                peer,
+
+        def in_plane():
+            for i, peer in enumerate(plane_peers):
+                launch(
+                    partial.at[at, beside(i)[0], beside(i)[1]],
+                    arrived.at[at, i],
+                    p_s.at[at, i],
+                    p_r.at[at, i],
+                    peer,
+                )
+
+        def straight():
+            for i in range(len(around)):
+                launch(
+                    partial.at[at, beside(i)[0], beside(i)[1]],
+                    arrived.at[z, i],
+                    p_s.at[at, i],
+                    p_r.at[z, i],
+                    device(at, *beside(i), core),
+                )
+            launch(
+                partial.at[at, y, x],
+                returned.at[z],
+                b_s.at[0 if at == 0 else zs - 2],
+                b_r.at[z],
+                device(at, y, x, core),
             )
+
+        if direct and at in (0, last):
+            pl.when(z == last - at)(straight)
+            unless(z == last - at, in_plane)
+        else:
+            in_plane()
 
     for at in range(zs):
         branches(at)
@@ -465,19 +561,42 @@
             value = value + arrived[at, i].astype(f32)
         return value
 
-    for k, peer in enumerate(z_peers):
-        if k == zs - 2:
-            combined = combined + plane_sum(z)
+    def homeward(k):
         summed[k] = plane_sum(planes[k]).astype(bf16)
-        send(summed.at[k], returned.at[z], b_s.at[k], b_r.at[z], peer)
-    if zs == 1:
-        combined = combined + plane_sum(z)
+        launch(summed.at[k], returned.at[z], b_s.at[k], b_r.at[z], z_peers[k])
+
+    for k in range(zs - 1):
+        if k == 0:
+            unless(z == last, functools.partial(homeward, k))
+        elif k == zs - 2:
+            unless(z == 0, functools.partial(homeward, k))
+        else:
+            homeward(k)
+    total[...] = combined + plane_sum(z)
+
+    def far_sum():
+        value = total[...]
+        for i in range(len(around)):
+            landed(arrived.at[far, i], p_r.at[far, i])
+            value = value + arrived[far, i].astype(f32)
+        total[...] = value
+
+    if direct:
+        pl.when(at_end)(far_sum)
+    combined = total[...]
     for plane in reversed(planes):
         landed(returned.at[plane], b_r.at[plane])
         combined = combined + returned[plane].astype(f32)
     out_ref[...] = (residual + combined * inverse_rms(combined)).astype(bf16)
-    for copy in started:
+    for copy in started + swap_copies():
         copy.wait_send()
+    for at in range(zs):
+        for i in range(len(around)):
+            drained(partial.at[at, y, x], p_s.at[at, i])
+            for q in range(2):
+                drained(piece(at, q), d_s.at[q, at, i])
+    for k in range(zs - 1):
+        drained(partial.at[0, y, x], b_s.at[k])
 
 
 def finish(a_ref, b_ref, c_ref, a_out, b_out, c_out, sems):
@@ -516,6 +635,7 @@
         pltpu.VMEM((zs, others, seq_count, width), bf16),
         pltpu.VMEM((z1, seq_count, width), bf16),
         pltpu.VMEM((zs, seq_count, width), bf16),
+        pltpu.VMEM((seq_count, width), f32),
     ]
     sems = [(9 * seq_count,), (6,), (6,)]
     sems += [(z1,), (zs,), (others,), (others,), (2, z1), (2, zs)]

time: 31.9 us -> 31.3 us (0.981)
  the two profiles are of different devices: /device:TPU:0 before, /device:TPU:16 now
where the time goes in v4:
time: 31.3 us; the launch traced here: 31.2 us
  Pallas kernels  30.5 us (97%)
  between operations  0.65 us (2%)
    pallas_call x1, Pallas kernels, whole_layer(): pl.pallas_call(functools.partial(layer, dims, head_count, expert_count),...  29.9 us
    pallas_call x1, Pallas kernels, whole_layer(): pl.pallas_call(finish, out_shape=[jax.ShapeDtypeStruct(shape, bf16) for s...  0.66 us

profile of v4, /device:TPU:16, one launch (start us, length us, event | category | flops | bytes accessed | tf_op | source)
XLA Modules:
  0.0 31.2 jit_solution(16035804716947924079)
XLA Ops:
  0.6 29.9 %shard_map.238 = (bf16[16,1024]{1,0:T(8,128)(2,1)S(1)}, bf16[16,512]{1,0:T(8,128)(2,1)S(1)}, bf16[16,1024]{1,0:T(8,128)(2,1)S(1)}) custom-call(bf16[16,1024]{1,0:T(8,128)(2,1)} %tokens_hbm.1, s32[1,16]{1,0:T(1,128)} %bitcast.11, s32[6,16]{1,0:T(8,128)} %bitcast.6, f32[6,16]{1,0:T(8,128)} %bitcast.7, f32[1,1024]{1,0:T(1,128)} %bitcast.8, f32[1,1024]{1,0:T(1,128)} %bitcast.9, ...), custom_call_target="tpu_custom_call" | custom-call | tf_op jit(solution)/shard_map/pallas_call | solution.py:644
  30.5 0.7 %shard_map.239 = (bf16[16,1024]{1,0:T(8,128)(2,1)}, bf16[16,512]{1,0:T(8,128)(2,1)}, bf16[16,1024]{1,0:T(8,128)(2,1)}) custom-call(bf16[16,1024]{1,0:T(8,128)(2,1)S(1)} %get-tuple-element.6.a_ref, bf16[16,512]{1,0:T(8,128)(2,1)S(1)} %get-tuple-element.7.b_ref, bf16[16,1024]{1,0:T(8,128)(2,1)S(1)} %get-tuple-element.8.c_ref), custom_call_target="tpu_custom_call" | custom-call | tf_op jit(solution)/shard_map/pallas_call | solution.py:654
